TPU v7x, 32 devices: a whole 2x2x4 slice. The times are simulated.
32 devices in a mesh: fs: 8 (over z, x), tp: 4 (over y, core).
Axes of the slice: x: 2, y: 2, z: 4, core: 2. Of those that a mesh axis runs over, the one named last changes fastest.
Arguments:
- normed_input: bfloat16 [16384, 2048], P('fs'), may hold values from -6 to 6
- gate_cotangent: bfloat16 [16384, 2048], P('fs', 'tp'), may hold values from -0.125 to 0.125
- first_value_cot: bfloat16 [16384, 1024], P('fs', 'tp'), may hold values from -0.125 to 0.125
- second_value_cot: bfloat16 [16384, 1024], P('fs', 'tp'), may hold values from -0.125 to 0.125
- head_lambda: float32 [8], P('tp'), may hold values from 0.3 to 0.8
- projection: bfloat16 [2048, 256], replicated, may hold values from -1 to 1, as said below
- gate_weight: float32 [2048, 2048], P('fs', 'tp'), may hold values from -0.125 to 0.125
- gate_first: float32 [256, 2048], P('fs', 'tp'), may hold values from -1.5 to 1.5
- gate_second: float32 [256, 2048], P('fs', 'tp'), may hold values from 0.01 to 1
- value_weight: float32 [2048, 1024], P('fs', 'tp'), may hold values from -0.125 to 0.125
- value_first: float32 [256, 1024], P('fs', 'tp'), may hold values from -1.5 to 1.5
- value_second: float32 [256, 1024], P('fs', 'tp'), may hold values from 0.01 to 1
Outputs:
- new_gate_weight: float32 [2048, 2048], P('fs', 'tp')
- gate_step: float32 [2048, 2048], P('fs', 'tp')
- gate_copy: bfloat16 [2048, 2048], P(None, 'tp')
- new_gate_first: float32 [256, 2048], P('fs', 'tp')
- new_gate_second: float32 [256, 2048], P('fs', 'tp')
- new_value_weight: float32 [2048, 1024], P('fs', 'tp')
- value_step: float32 [2048, 1024], P('fs', 'tp')
- value_copy: bfloat16 [2048, 1024], P(None, 'tp')
- new_value_first: float32 [256, 1024], P('fs', 'tp')
- new_value_second: float32 [256, 1024], P('fs', 'tp')
Inputs may be any that keep to these rules, and one draw needn't show every extreme that they name: `projection`: a low-rank factor whose rows differ in scale.
All inputs are finite; a program needn't handle non-finite values.
Results may differ from a plain program's by a relative error of at most 0.0054.
Values may be sent and summed in bfloat16 or wider, within the bound.
A program may use at most 64 MiB of HBM per device.

v0:
```python
import functools

import jax
import jax.numpy as jnp
from jax import lax
from jax.experimental import pallas as pl
from jax.experimental.pallas import tpu as pltpu
from jax.sharding import PartitionSpec as P

VDIM = 128
PIECES = 4
CHUNKS = 4
STEP_TOKENS = 256

moment_decay = 0.9
square_decay = 0.95
adam_floor = 1e-08
learn_rate = 0.02
rms_floor = 0.1

MESH = pl.DeviceIdType.MESH
f32, bf16 = jnp.float32, jnp.bfloat16


def factor_fs(count):
    inner = 1
    while (2 * inner) ** 2 <= count and count % (2 * inner) == 0:
        inner *= 2
    return count // inner, inner


def kernel(
    nz,
    nx,
    nt,
    x_hbm,
    gcot_hbm,
    fcot_hbm,
    scot_hbm,
    lam_ref,
    proj_hbm,
    gw_hbm,
    gm_hbm,
    gs_hbm,
    vw_hbm,
    vm_hbm,
    vs_hbm,
    wall_hbm,
    dir_hbm,
    scale_hbm,
    ngm_hbm,
    ngs_hbm,
    nvm_hbm,
    nvs_hbm,
    xv,
    gcv,
    fcv,
    scv,
    pv,
    gw,
    vw,
    gm,
    gs,
    vm,
    vs,
    wall,
    acc,
    rsrc,
    rsx,
    zsrc,
    rsz,
    dall,
    dcat,
    direct,
    sums,
    scales,
    in_sem,
    x_sem,
    out_sem,
    copy_sem,
    wz_send,
    wz_recv,
    wx_send,
    wx_recv,
    rx_send,
    rx_recv,
    rz_send,
    rz_recv,
    dz_send,
    dz_recv,
    dx_send,
    dx_recv,
    t_send,
    t_recv,
):
    nfs = nz * nx
    f = lax.axis_index("fs")
    t = lax.axis_index("tp")
    z = lax.div(f, nx)
    x = lax.rem(f, nx)
    rows, cg = gw.shape
    cv = vw.shape[1]
    cols = cg + cv
    rank = acc.shape[0]
    share = rank // nfs
    part = rows // PIECES
    tokens = x_hbm.shape[0] // CHUNKS

    def zpeer(k):
        return lax.rem(z + k, nz)

    def xpeer(k):
        return lax.rem(x + k, nx)

    barrier = pltpu.get_barrier_semaphore()
    for k in range(1, nz):
        pl.semaphore_signal(barrier, inc=1, device_id=(zpeer(k) * nx + x, t), device_id_type=MESH)
    for k in range(1, nx):
        pl.semaphore_signal(barrier, inc=1, device_id=(z * nx + xpeer(k), t), device_id_type=MESH)
    for k in range(1, nt):
        pl.semaphore_signal(barrier, inc=1, device_id=(f, lax.rem(t + k, nt)), device_id_type=MESH)

    small = [
        pltpu.make_async_copy(src, dst, in_sem.at[i])
        for i, (src, dst) in enumerate(
            [
                (gw_hbm, gw),
                (vw_hbm, vw),
                (proj_hbm, pv),
                (gm_hbm, gm),
                (gs_hbm, gs),
                (vm_hbm, vm),
                (vs_hbm, vs),
            ]
        )
    ]

    def chunk_copies(c):
        at = pl.ds(c * tokens, tokens)
        return [
            pltpu.make_async_copy(src.at[at], dst.at[at], x_sem.at[i, c])
            for i, (src, dst) in enumerate(
                [(x_hbm, xv), (gcot_hbm, gcv), (fcot_hbm, fcv), (scot_hbm, scv)]
            )
        ]

    for i in range(3):
        small[i].start()
    for c in range(CHUNKS):
        for copy in chunk_copies(c):
            copy.start()
    for i in range(3, 7):
        small[i].start()

    small[0].wait()
    small[1].wait()
    for p in range(PIECES):
        at = pl.ds(p * part, part)
        wall[f, p, :, :cg] = gw[at, :].astype(bf16)
        wall[f, p, :, cg:] = vw[at, :].astype(bf16)

    def wz(k, p, src_z):
        owner = src_z * nx + x
        return pltpu.make_async_remote_copy(
            src_ref=wall.at[owner, p],
            dst_ref=wall.at[owner, p],
            send_sem=wz_send.at[k, p],
            recv_sem=wz_recv.at[src_z, p],
            device_id=(zpeer(k) * nx + x, t),
            device_id_type=MESH,
        )

    def wx(k, p, src_z, src_x):
        owner = src_z * nx + src_x
        return pltpu.make_async_remote_copy(
            src_ref=wall.at[owner, p],
            dst_ref=wall.at[owner, p],
            send_sem=wx_send.at[k, src_z, p],
            recv_sem=wx_recv.at[src_x, src_z, p],
            device_id=(z * nx + xpeer(k), t),
            device_id_type=MESH,
        )

    def send_z(p):
        for k in range(1, nz):
            wz(k, p, z).start()

    def relay(p):
        for k in range(1, nz):
            wz(k, p, zpeer(k)).wait_recv()
            for m in range(1, nx):
                wx(m, p, zpeer(k), x).start()

    pl.semaphore_wait(barrier, (nz - 1) + (nx - 1) + (nt - 1))
    send_z(0)
    for p in range(PIECES):
        for k in range(1, nx):
            wx(k, p, z, x).start()

    small[2].wait()
    acc[...] = jnp.zeros_like(acc)
    head = lax.broadcasted_iota(jnp.int32, (1, cv), 1) // VDIM
    lam = jnp.zeros((1, cv), f32)
    for h in range(cv // VDIM):
        lam = jnp.where(head == h, lam_ref[h], lam)
    for c in range(CHUNKS):
        for copy in chunk_copies(c):
            copy.wait()

        def multiply(i, carry):
            at = pl.ds(pl.multiple_of(c * tokens + i * STEP_TOKENS, STEP_TOKENS), STEP_TOKENS)
            upper = jnp.dot(xv[at, :], pv[...], preferred_element_type=f32).astype(bf16)
            value = (fcv[at, :].astype(f32) - lam * scv[at, :].astype(f32)).astype(bf16)
            over = (((0,), (0,)), ((), ()))
            acc[:, :cg] += lax.dot_general(upper, gcv[at, :], over, preferred_element_type=f32)
            acc[:, cg:] += lax.dot_general(upper, value, over, preferred_element_type=f32)
            return carry

        lax.fori_loop(0, tokens // STEP_TOKENS, multiply, 0)

    for zi in range(nz):
        for xi in range(nx):
            at = pl.ds((zi * nx + xi) * share, share)
            rsrc[xi, zi] = acc[at, :].astype(bf16)

    def rx(k, src_x, dst_x):
        return pltpu.make_async_remote_copy(
            src_ref=rsrc.at[dst_x],
            dst_ref=rsx.at[src_x],
            send_sem=rx_send.at[k],
            recv_sem=rx_recv.at[src_x],
            device_id=(z * nx + xpeer(k), t),
            device_id_type=MESH,
        )

    for k in range(1, nx):
        rx(k, x, xpeer(k)).start()
    send_z(1)
    relay(0)
    for k in range(1, nx):
        rx(k, xpeer(k), x).wait_recv()
    for zi in range(nz):
        at = pl.ds(pl.multiple_of((zi * nx + x) * share, share), share)
        total = acc[at, :]
        for k in range(1, nx):
            total = total + rsx[xpeer(k), zi].astype(f32)
        zsrc[zi] = total.astype(bf16)

    def rz(k, src_z, dst_z):
        return pltpu.make_async_remote_copy(
            src_ref=zsrc.at[dst_z],
            dst_ref=rsz.at[src_z],
            send_sem=rz_send.at[k],
            recv_sem=rz_recv.at[src_z],
            device_id=(zpeer(k) * nx + x, t),
            device_id_type=MESH,
        )

    for k in range(1, nz):
        rz(k, z, zpeer(k)).start()
    relay(1)
    for i in range(3, 7):
        small[i].wait()
    low = zsrc[z].astype(f32)
    for k in range(1, nz):
        rz(k, zpeer(k), z).wait_recv()
        low = low + rsz[zpeer(k)].astype(f32)

    for first, second, at in ((gm, gs, slice(0, cg)), (vm, vs, slice(cg, cols))):
        mine = low[:, at]
        new_first = moment_decay * first[...] + (1.0 - moment_decay) * mine
        new_second = square_decay * second[...] + (1.0 - square_decay) * mine * mine
        first[...] = new_first
        second[...] = new_second
        dall[f, :, at] = (new_first / (jnp.sqrt(new_second) + adam_floor)).astype(bf16)

    outs = [
        pltpu.make_async_copy(src, dst, out_sem.at[i])
        for i, (src, dst) in enumerate(
            [
                (gm, ngm_hbm),
                (gs, ngs_hbm),
                (vm, nvm_hbm),
                (vs, nvs_hbm),
                (direct, dir_hbm),
                (scales, scale_hbm),
            ]
        )
    ]
    for i in range(4):
        outs[i].start()

    def dz(k, src_z):
        owner = src_z * nx + x
        return pltpu.make_async_remote_copy(
            src_ref=dall.at[owner],
            dst_ref=dall.at[owner],
            send_sem=dz_send.at[k],
            recv_sem=dz_recv.at[src_z],
            device_id=(zpeer(k) * nx + x, t),
            device_id_type=MESH,
        )

    def dx(k, src_z, src_x):
        owner = src_z * nx + src_x
        return pltpu.make_async_remote_copy(
            src_ref=dall.at[owner],
            dst_ref=dall.at[owner],
            send_sem=dx_send.at[k, src_z],
            recv_sem=dx_recv.at[src_x, src_z],
            device_id=(z * nx + xpeer(k), t),
            device_id_type=MESH,
        )

    for k in range(1, nz):
        dz(k, z).start()
    for m in range(1, nx):
        dx(m, z, x).start()
    send_z(2)
    send_z(3)
    for k in range(1, nz):
        dz(k, zpeer(k)).wait_recv()
        for m in range(1, nx):
            dx(m, zpeer(k), x).start()
    for m in range(1, nx):
        for zi in range(nz):
            dx(m, zi, xpeer(m)).wait_recv()

    relay(2)
    relay(3)
    for j in range(nfs):
        dcat[pl.ds(j * share, share), :] = dall[j].astype(f32)
    direction = dcat[...].astype(bf16)
    direct[...] = direction
    outs[4].start()

    def expand(j, squares):
        left = pv[pl.ds(pl.multiple_of(j * rows, rows), rows), :]
        block = jnp.dot(left, direction, preferred_element_type=f32)
        return squares + jnp.sum(block * block, axis=0, keepdims=True)

    squares = lax.fori_loop(0, nfs, expand, jnp.zeros((1, cols), f32))
    gate_sum = jnp.sum(squares[:, :cg], axis=1, keepdims=True)
    value_sum = jnp.sum(squares[:, cg:], axis=1, keepdims=True)
    sums[t, 0] = jnp.broadcast_to(gate_sum, (8, 128))
    sums[t, 1] = jnp.broadcast_to(value_sum, (8, 128))

    def tp(k, src_t):
        return pltpu.make_async_remote_copy(
            src_ref=sums.at[src_t],
            dst_ref=sums.at[src_t],
            send_sem=t_send.at[k],
            recv_sem=t_recv.at[src_t],
            device_id=(f, lax.rem(t + k, nt)),
            device_id_type=MESH,
        )

    for k in range(1, nt):
        tp(k, t).start()
    for k in range(1, nt):
        tp(k, lax.rem(t + k, nt)).wait_recv()
    whole = sums[0]
    for k in range(1, nt):
        whole = whole + sums[k]
    entries = nfs * rows * nt
    scales[0] = 1.0 / (jnp.sqrt(whole[0] / (entries * cg)) + rms_floor)
    scales[1] = 1.0 / (jnp.sqrt(whole[1] / (entries * cv)) + rms_floor)
    outs[5].start()

    copies = []
    for p in range(PIECES):
        for m in range(1, nx):
            for zi in range(nz):
                wx(m, p, zi, xpeer(m)).wait_recv()
        copies.append(pltpu.make_async_copy(wall.at[:, p], wall_hbm.at[:, p], copy_sem.at[p]))
        copies[-1].start()

    for copy in copies + outs:
        copy.wait()
    for k in range(1, nz):
        for p in range(PIECES):
            wz(k, p, z).wait_send()
        rz(k, z, zpeer(k)).wait_send()
        dz(k, z).wait_send()
    for m in range(1, nx):
        rx(m, x, xpeer(m)).wait_send()
        for zi in range(nz):
            for p in range(PIECES):
                wx(m, p, zi, x).wait_send()
            dx(m, zi, x).wait_send()
    for k in range(1, nt):
        tp(k, t).wait_send()


def finish_kernel(
    nz,
    nx,
    proj_hbm,
    gw_hbm,
    vw_hbm,
    wall,
    dir_hbm,
    scale_ref,
    ngm_hbm,
    ngs_hbm,
    nvm_hbm,
    nvs_hbm,
    ngw_out,
    gstep_out,
    gcopy_out,
    ngm_out,
    ngs_out,
    nvw_out,
    vstep_out,
    vcopy_out,
    nvm_out,
    nvs_out,
    pv,
    gw,
    vw,
    direct,
    gm,
    gs,
    vm,
    vs,
    gcs,
    vcs,
    gsteps,
    vsteps,
    in_sem,
    out_sem,
    copy_sem,
):
    nfs = nz * nx
    f = lax.axis_index("fs")
    rows, cg = gw.shape
    moments = [(ngm_hbm, gm, ngm_out), (ngs_hbm, gs, ngs_out), (nvm_hbm, vm, nvm_out), (nvs_hbm, vs, nvs_out)]
    loads = [(dir_hbm, direct), (proj_hbm, pv), (gw_hbm, gw), (vw_hbm, vw)]
    loads += [(src, held) for src, held, _ in moments]
    loads = [pltpu.make_async_copy(src, dst, in_sem.at[i]) for i, (src, dst) in enumerate(loads)]
    stores = [(held, dst) for _, held, dst in moments]
    stores += [(gw, ngw_out), (vw, nvw_out), (gsteps, gstep_out), (vsteps, vstep_out)]
    stores = [pltpu.make_async_copy(src, dst, out_sem.at[i]) for i, (src, dst) in enumerate(stores)]

    def put(j):
        return [
            pltpu.make_async_copy(gcs.at[j], gcopy_out.at[j], copy_sem.at[0, j]),
            pltpu.make_async_copy(vcs.at[j], vcopy_out.at[j], copy_sem.at[1, j]),
        ]

    for i in range(2):
        loads[i].start()
    for i in range(2, 8):
        loads[i].start()
    gscale = scale_ref[0, 0:1, 0:1]
    vscale = scale_ref[1, 0:1, 0:1]
    for i in range(2):
        loads[i].wait()
    direction = direct[...]

    def block(j):
        left = pv[pl.ds(pl.multiple_of(j * rows, rows), rows), :]
        return jnp.dot(left, direction, preferred_element_type=f32)

    def finish(j, carry):
        update = block(j)
        held = wall[j].astype(f32).reshape(update.shape)
        gcs[j] = (held[:, :cg] - learn_rate * (update[:, :cg] * gscale)).astype(bf16)
        vcs[j] = (held[:, cg:] - learn_rate * (update[:, cg:] * vscale)).astype(bf16)
        for copy in put(j):
            copy.start()
        return carry

    lax.fori_loop(0, nfs, finish, 0)
    for i in range(2, 8):
        loads[i].wait()
    for i in range(4):
        stores[i].start()
    mine = block(f)
    gstep = mine[:, :cg] * gscale
    vstep = mine[:, cg:] * vscale
    gsteps[...] = gstep
    vsteps[...] = vstep
    gw[...] = gw[...] - learn_rate * gstep
    vw[...] = vw[...] - learn_rate * vstep
    for i in range(4, 8):
        stores[i].start()
    for j in range(nfs):
        for copy in put(j):
            copy.wait()
    for copy in stores:
        copy.wait()


def per_device(nz, nx, nt, xin, gcot, fcot, scot, lam, proj, gw, gm, gs, vw, vm, vs):
    nfs = nz * nx
    rows, cg = gw.shape
    cv = vw.shape[1]
    cols = cg + cv
    depth, rank = proj.shape
    share = rank // nfs
    part = rows // PIECES
    anywhere = pl.BlockSpec(memory_space=pl.ANY)
    pinned = pl.BlockSpec(memory_space=pl.ANY)
    dma = pltpu.SemaphoreType.DMA
    shape = jax.ShapeDtypeStruct
    like = lambda a: shape(a.shape, a.dtype)
    vmem = lambda a: pltpu.VMEM(a.shape, a.dtype)
    wall, direction, scale, *moments = pl.pallas_call(
        functools.partial(kernel, nz, nx, nt),
        out_shape=[
            shape((nfs, PIECES, part, cols), bf16),
            shape((rank, cols), bf16),
            shape((2, 8, 128), f32),
            like(gm),
            like(gs),
            like(vm),
            like(vs),
        ],
        in_specs=[pinned] * 4 + [pl.BlockSpec(memory_space=pltpu.SMEM)] + [pinned] * 7,
        out_specs=[anywhere] * 7,
        scratch_shapes=[
            vmem(xin),
            vmem(gcot),
            vmem(fcot),
            vmem(scot),
            vmem(proj),
            vmem(gw),
            vmem(vw),
            vmem(gm),
            vmem(gs),
            vmem(vm),
            vmem(vs),
            pltpu.VMEM((nfs, PIECES, part, cols), bf16),
            pltpu.VMEM((rank, cols), f32),
            pltpu.VMEM((nx, nz, share, cols), bf16),
            pltpu.VMEM((nx, nz, share, cols), bf16),
            pltpu.VMEM((nz, share, cols), bf16),
            pltpu.VMEM((nz, share, cols), bf16),
            pltpu.VMEM((nfs, share, cols), bf16),
            pltpu.VMEM((rank, cols), f32),
            pltpu.VMEM((rank, cols), bf16),
            pltpu.VMEM((nt, 2, 8, 128), f32),
            pltpu.VMEM((2, 8, 128), f32),
            dma((7,)),
            dma((4, CHUNKS)),
            dma((6,)),
            dma((PIECES,)),
            dma((nz, PIECES)),
            dma((nz, PIECES)),
            dma((nx, nz, PIECES)),
            dma((nx, nz, PIECES)),
            dma((nx,)),
            dma((nx,)),
            dma((nz,)),
            dma((nz,)),
            dma((nz,)),
            dma((nz,)),
            dma((nx, nz)),
            dma((nx, nz)),
            dma((nt,)),
            dma((nt,)),
        ],
        compiler_params=pltpu.CompilerParams(
            collective_id=0, has_side_effects=True, vmem_limit_bytes=60 * 1024 * 1024
        ),
    )(xin, gcot, fcot, scot, lam, proj, gw, gm, gs, vw, vm, vs)
    results = pl.pallas_call(
        functools.partial(finish_kernel, nz, nx),
        out_shape=[
            like(gw),
            like(gw),
            shape((nfs, rows, cg), bf16),
            like(gm),
            like(gs),
            like(vw),
            like(vw),
            shape((nfs, rows, cv), bf16),
            like(vm),
            like(vs),
        ],
        in_specs=[pinned] * 3 + [pl.BlockSpec(memory_space=pltpu.VMEM), anywhere] + [pl.BlockSpec(memory_space=pltpu.VMEM)] + [anywhere] * 4,
        out_specs=[anywhere] * 10,
        scratch_shapes=[
            vmem(proj),
            vmem(gw),
            vmem(vw),
            vmem(direction),
            vmem(gm),
            vmem(gs),
            vmem(vm),
            vmem(vs),
            pltpu.VMEM((nfs, rows, cg), bf16),
            pltpu.VMEM((nfs, rows, cv), bf16),
            vmem(gw),
            vmem(vw),
            dma((8,)),
            dma((8,)),
            dma((2, nfs)),
        ],
        compiler_params=pltpu.CompilerParams(vmem_limit_bytes=60 * 1024 * 1024),
    )(proj, gw, vw, wall, direction, scale, *moments)
    results = list(results)
    results[2] = results[2].reshape(depth, cg)
    results[7] = results[7].reshape(depth, cv)
    return tuple(results)


def solution(mesh):
    nz, nx = factor_fs(mesh.shape["fs"])
    split, whole = P("fs", "tp"), P(None, "tp")
    placed = (P("fs", None), split, split, split, P("tp"), P()) + (split,) * 6
    return jax.shard_map(
        functools.partial(per_device, nz, nx, mesh.shape["tp"]),
        mesh=mesh,
        in_specs=placed,
        out_specs=(split, split, whole, split, split, split, split, whole, split, split),
        check_vma=False,
    )
```

profile of v0, /device:TPU:12, one launch (start us, length us, event | category | flops | bytes accessed | tf_op | source)
XLA Modules:
  0.0 69.1 jit_solution(14173665450648370555)
XLA Ops:
  0.6 61.1 %shard_map.195 = (bf16[8,4,64,768]{3,2,1,0:T(8,128)(2,1)}, bf16[256,768]{1,0:T(8,128)(2,1)}, f32[2,8,128]{2,1,0:T(8,128)}, f32[32,512]{1,0:T(8,128)}, f32[32,512...) custom-call(bf16[2048,2048]{1,0:T(8,128)(2,1)} %x_hbm.1, bf16[2048,512]{1,0:T(8,128)(2,1)} %gcot_hbm.1, ...), custom_call_target="tpu_custom_call" | custom-call | tf_op jit(solution)/shard_map/pallas_call | solution.py:509
  61.8 7.4 %shard_map.196 = (f32[256,512]{1,0:T(8,128)}, f32[256,512]{1,0:T(8,128)}, bf16[8,256,512]{2,1,0:T(8,128)(2,1)}, f32[32,512]{1,0:T(8,128)}, f32[32,512]{1,0:T(8,1...) custom-call(bf16[2048,256]{1,0:T(8,128)(2,1)} %proj_hbm.3, ...), custom_call_target="tpu_custom_call" | custom-call | tf_op jit(solution)/shard_map/pallas_call | solution.py:568
where the time goes:
time: 69.3 us; the launch traced here: 69.1 us
  Pallas kernels  68.5 us (99%)
    pallas_call x1, Pallas kernels, per_device(): pl.pallas_call(functools.partial(kernel, nz, nx, nt), out_shape=[shape((n...  61.1 us
    pallas_call x1, Pallas kernels, per_device(): pl.pallas_call(functools.partial(finish_kernel, nz, nx), out_shape=[like(...  7.37 us

commit v1 on v0

v1 whole, which is shorter than its diff:
```python
import functools

import jax
import jax.numpy as jnp
from jax import lax
from jax.experimental import pallas as pl
from jax.experimental.pallas import tpu as pltpu
from jax.sharding import PartitionSpec as P

VDIM = 128
PIECES = 8
PIECE_ROWS = 16
CROSS = 1
CHUNKS = 4
STEP_TOKENS = 256
HOLD_X = 4
HOLD_ONE = 6
HOLD_TWO = 4
HOLD_THREE = 4

moment_decay = 0.9
square_decay = 0.95
adam_floor = 1e-08
learn_rate = 0.02
rms_floor = 0.1

MESH = pl.DeviceIdType.MESH
f32, bf16 = jnp.float32, jnp.bfloat16


def factor_fs(count):
    inner = 1
    while (2 * inner) ** 2 <= count and count % (2 * inner) == 0:
        inner *= 2
    return count // inner, inner


def kernel(
    nz,
    nx,
    nt,
    x_hbm,
    gcot_hbm,
    fcot_hbm,
    scot_hbm,
    lam_hbm,
    proj_hbm,
    gw_hbm,
    gm_hbm,
    gs_hbm,
    vw_hbm,
    vm_hbm,
    vs_hbm,
    new_gw,
    gsteps,
    gcopy,
    new_gm,
    new_gs,
    new_vw,
    vsteps,
    vcopy,
    new_vm,
    new_vs,
    lam_ref,
    xv,
    gcv,
    fcv,
    scv,
    pv,
    gw,
    vw,
    gm,
    gs,
    vm,
    vs,
    wall,
    acc,
    updates,
    rsrc,
    rsx,
    zsrc,
    rsz,
    dall,
    dcat,
    sums,
    in_sem,
    x_sem,
    wz_send,
    wz_recv,
    wx_send,
    wx_recv,
    rx_send,
    rx_recv,
    rz_send,
    rz_recv,
    dz_send,
    dz_recv,
    dx_send,
    dx_recv,
    t_send,
    t_recv,
):
    nfs = nz * nx
    f = lax.axis_index("fs")
    t = lax.axis_index("tp")
    z = lax.div(f, nx)
    x = lax.rem(f, nx)
    rows, cg = gw.shape
    cv = vw.shape[1]
    cols = cg + cv
    rank = acc.shape[0]
    share = rank // nfs
    pieces, part = wall.shape[1:3]
    tokens = x_hbm.shape[0] // CHUNKS
    cross = range(pieces * CROSS // 8)
    direct = range(len(cross), pieces)
    items = [(0, p) for p in range(pieces)] + [(k, p) for p in cross for k in range(1, nx)]

    def zpeer(k):
        return lax.rem(z + k, nz)

    def xpeer(k):
        return lax.rem(x + k, nx)

    barrier = pltpu.get_barrier_semaphore()
    for k in range(1, nz):
        pl.semaphore_signal(barrier, inc=1, device_id=(zpeer(k) * nx + x, t), device_id_type=MESH)
    for k in range(1, nx):
        pl.semaphore_signal(barrier, inc=1, device_id=(z * nx + xpeer(k), t), device_id_type=MESH)
    for k in range(1, nt):
        pl.semaphore_signal(barrier, inc=1, device_id=(f, lax.rem(t + k, nt)), device_id_type=MESH)

    small = [
        pltpu.make_async_copy(src, dst, in_sem.at[i])
        for i, (src, dst) in enumerate(
            [
                (gw_hbm, gw),
                (vw_hbm, vw),
                (proj_hbm, pv),
                (gm_hbm, gm),
                (gs_hbm, gs),
                (vm_hbm, vm),
                (vs_hbm, vs),
                (lam_hbm, lam_ref),
            ]
        )
        if src is not lam_hbm or cv > VDIM
    ]
    if cv == VDIM:
        lam_ref = lam_hbm

    def chunk_copies(c):
        at = pl.ds(c * tokens, tokens)
        return [
            pltpu.make_async_copy(src.at[at], dst.at[at], x_sem.at[i, c])
            for i, (src, dst) in enumerate(
                [(x_hbm, xv), (gcot_hbm, gcv), (fcot_hbm, fcv), (scot_hbm, scv)]
            )
        ]

    for copy in small[:3] + small[7:]:
        copy.start()
    for c in range(CHUNKS):
        for copy in chunk_copies(c):
            copy.start()
    for i in range(3, 7):
        small[i].start()

    small[0].wait()
    small[1].wait()
    for p in range(pieces):
        at = pl.ds(p * part, part)
        wall[f, p, :, :cg] = gw[at, :].astype(bf16)
        wall[f, p, :, cg:] = vw[at, :].astype(bf16)

    def valid(row):
        return jnp.logical_and(row >= 0, row < nz)

    def wz(way, src_z, i, peer):
        k, p = items[i]
        owner = src_z * nx + xpeer(k)
        return pltpu.make_async_remote_copy(
            src_ref=wall.at[owner, p],
            dst_ref=wall.at[owner, p],
            send_sem=wz_send.at[(way + 1) // 2, src_z, i],
            recv_sem=wz_recv.at[src_z, i],
            device_id=(peer * nx + x, t),
            device_id_type=MESH,
        )

    def wx(k, p, src_z, src_x):
        owner = src_z * nx + src_x
        return pltpu.make_async_remote_copy(
            src_ref=wall.at[owner, p],
            dst_ref=wall.at[owner, p],
            send_sem=wx_send.at[k, src_z, p],
            recv_sem=wx_recv.at[src_x, src_z, p],
            device_id=(z * nx + xpeer(k), t),
            device_id_type=MESH,
        )

    def along(way, src_z, i):
        @pl.when(valid(z + way))
        def _():
            wz(way, src_z, i, z + way).start()

    def over(src_z, p):
        for k in range(1, nx):
            wx(k, p, src_z, x).start()

    def relay(step, i):
        k, p = items[i]
        for way in (1, -1):
            src_z = z - way * step

            @pl.when(valid(src_z))
            def _():
                wz(way, src_z, i, z - way).wait_recv()
                along(way, src_z, i)
                if k == 0 and p in direct:
                    over(src_z, p)

    def cross_over():
        for i in range(pieces, len(items)):
            k, p = items[i]
            wx(k, p, z, xpeer(k)).wait_recv()
            for way in (1, -1):
                along(way, z, i)

    pl.semaphore_wait(barrier, (nz - 1) + (nx - 1) + (nt - 1))
    for p in cross:
        over(z, p)
    for p in range(pieces):
        for way in (1, -1):
            along(way, z, p)
        if p in direct and p < HOLD_X:
            over(z, p)

    for copy in small[2:3] + small[7:]:
        copy.wait()
    acc[...] = jnp.zeros_like(acc)
    head = lax.broadcasted_iota(jnp.int32, (1, cv), 1) // VDIM
    lam = jnp.zeros((1, cv), f32)
    for h in range(cv // VDIM):
        lam = jnp.where(head == h, lam_ref[h], lam)
    for c in range(CHUNKS):
        for copy in chunk_copies(c):
            copy.wait()

        def multiply(i, carry):
            at = pl.ds(pl.multiple_of(c * tokens + i * STEP_TOKENS, STEP_TOKENS), STEP_TOKENS)
            upper = jnp.dot(xv[at, :], pv[...], preferred_element_type=f32).astype(bf16)
            value = (fcv[at, :].astype(f32) - lam * scv[at, :].astype(f32)).astype(bf16)
            across = (((0,), (0,)), ((), ()))
            acc[:, :cg] += lax.dot_general(upper, gcv[at, :], across, preferred_element_type=f32)
            acc[:, cg:] += lax.dot_general(upper, value, across, preferred_element_type=f32)
            return carry

        lax.fori_loop(0, tokens // STEP_TOKENS, multiply, 0)

    for zi in range(nz):
        for xi in range(nx):
            at = pl.ds((zi * nx + xi) * share, share)
            rsrc[xi, zi] = acc[at, :].astype(bf16)

    def rx(k, src_x, dst_x):
        return pltpu.make_async_remote_copy(
            src_ref=rsrc.at[dst_x],
            dst_ref=rsx.at[src_x],
            send_sem=rx_send.at[k],
            recv_sem=rx_recv.at[src_x],
            device_id=(z * nx + xpeer(k), t),
            device_id_type=MESH,
        )

    for k in range(1, nx):
        rx(k, x, xpeer(k)).start()
    cross_over()
    for p in direct:
        if p >= HOLD_X:
            over(z, p)

    def relays(step, lo, hi):
        if step < nz:
            for i in range(min(lo, len(items)), min(hi, len(items))):
                relay(step, i)

    relays(1, 0, HOLD_ONE)
    for k in range(1, nx):
        rx(k, xpeer(k), x).wait_recv()
    for zi in range(nz):
        at = pl.ds(pl.multiple_of((zi * nx + x) * share, share), share)
        total = acc[at, :]
        for k in range(1, nx):
            total = total + rsx[xpeer(k), zi].astype(f32)
        zsrc[zi] = total.astype(bf16)

    def rz(k, src_z, dst_z):
        return pltpu.make_async_remote_copy(
            src_ref=zsrc.at[dst_z],
            dst_ref=rsz.at[src_z],
            send_sem=rz_send.at[k],
            recv_sem=rz_recv.at[src_z],
            device_id=(zpeer(k) * nx + x, t),
            device_id_type=MESH,
        )

    for k in range(1, nz):
        rz(k, z, zpeer(k)).start()
    relays(1, HOLD_ONE, len(items))
    relays(2, 0, HOLD_TWO)
    for i in range(3, 7):
        small[i].wait()
    low = zsrc[z].astype(f32)
    for k in range(1, nz):
        rz(k, zpeer(k), z).wait_recv()
        low = low + rsz[zpeer(k)].astype(f32)

    for first, second, new_m, new_s, at in (
        (gm, gs, new_gm, new_gs, slice(0, cg)),
        (vm, vs, new_vm, new_vs, slice(cg, cols)),
    ):
        mine = low[:, at]
        new_first = moment_decay * first[...] + (1.0 - moment_decay) * mine
        new_second = square_decay * second[...] + (1.0 - square_decay) * mine * mine
        new_m[...] = new_first
        new_s[...] = new_second
        dall[f, :, at] = (new_first / (jnp.sqrt(new_second) + adam_floor)).astype(bf16)

    def dz(k, src_z):
        owner = src_z * nx + x
        return pltpu.make_async_remote_copy(
            src_ref=dall.at[owner],
            dst_ref=dall.at[owner],
            send_sem=dz_send.at[k],
            recv_sem=dz_recv.at[src_z],
            device_id=(zpeer(k) * nx + x, t),
            device_id_type=MESH,
        )

    def dx(k, src_z, src_x):
        owner = src_z * nx + src_x
        return pltpu.make_async_remote_copy(
            src_ref=dall.at[owner],
            dst_ref=dall.at[owner],
            send_sem=dx_send.at[k, src_z],
            recv_sem=dx_recv.at[src_x, src_z],
            device_id=(z * nx + xpeer(k), t),
            device_id_type=MESH,
        )

    for k in range(1, nz):
        dz(k, z).start()
    for m in range(1, nx):
        dx(m, z, x).start()
    relays(2, HOLD_TWO, len(items))
    for k in range(1, nz):
        dz(k, zpeer(k)).wait_recv()
        for m in range(1, nx):
            dx(m, zpeer(k), x).start()
    relays(3, 0, HOLD_THREE)
    for m in range(1, nx):
        for zi in range(nz):
            dx(m, zi, xpeer(m)).wait_recv()

    for j in range(nfs):
        dcat[pl.ds(j * share, share), :] = dall[j].astype(f32)
    direction = dcat[...].astype(bf16)

    def expand(j, squares):
        at = pl.ds(pl.multiple_of(j * rows, rows), rows)
        block = jnp.dot(pv[at, :], direction, preferred_element_type=f32)
        updates[at, :] = block
        return squares + jnp.sum((block * block).reshape(rows // 8, 8, cols), axis=0)

    squares = lax.fori_loop(0, nfs, expand, jnp.zeros((8, cols), f32))
    squares = jnp.sum(squares, axis=0, keepdims=True)
    gate_sum = jnp.sum(squares[:, :cg], axis=1, keepdims=True)
    value_sum = jnp.sum(squares[:, cg:], axis=1, keepdims=True)
    sums[t, 0] = jnp.broadcast_to(gate_sum, (8, 128))
    sums[t, 1] = jnp.broadcast_to(value_sum, (8, 128))

    def tp(k, src_t):
        return pltpu.make_async_remote_copy(
            src_ref=sums.at[src_t],
            dst_ref=sums.at[src_t],
            send_sem=t_send.at[k],
            recv_sem=t_recv.at[src_t],
            device_id=(f, lax.rem(t + k, nt)),
            device_id_type=MESH,
        )

    for k in range(1, nt):
        tp(k, t).start()
    relays(3, HOLD_THREE, len(items))
    for step in range(4, nz):
        relays(step, 0, len(items))
    for k in range(1, nt):
        tp(k, lax.rem(t + k, nt)).wait_recv()
    whole = sums[0]
    for k in range(1, nt):
        whole = whole + sums[k]
    entries = nfs * rows * nt
    gscale = (1.0 / (jnp.sqrt(whole[0] / (entries * cg)) + rms_floor))[0:1, 0:1]
    vscale = (1.0 / (jnp.sqrt(whole[1] / (entries * cv)) + rms_floor))[0:1, 0:1]

    at = pl.ds(pl.multiple_of(f * rows, rows), rows)
    gstep = updates[at, :cg] * gscale
    vstep = updates[at, cg:] * vscale
    gsteps[...] = gstep
    vsteps[...] = vstep
    new_gw[...] = gw[...] - learn_rate * gstep
    new_vw[...] = vw[...] - learn_rate * vstep

    def finish(j, p):
        at = pl.ds(pl.multiple_of(j * rows + p * part, part), part)
        held = wall[j, p].astype(f32)
        update = updates[at, :]
        gcopy[at, :] = (held[:, :cg] - learn_rate * (update[:, :cg] * gscale)).astype(bf16)
        vcopy[at, :] = (held[:, cg:] - learn_rate * (update[:, cg:] * vscale)).astype(bf16)

    def finish_block(j, lo, hi):
        def body(p, carry):
            finish(j, p)
            return carry

        lax.fori_loop(lo, hi, body, 0)

    for zi in range(nz):
        finish_block(zi * nx + x, 0, pieces)
        if len(cross):
            for k in range(1, nx):
                finish_block(zi * nx + xpeer(k), 0, len(cross))
    for step in range(nz):
        for p in direct:
            for way in (1, -1) if step else (1,):
                src_z = z - way * step

                @pl.when(valid(src_z))
                def _():
                    for k in range(1, nx):
                        wx(k, p, src_z, xpeer(k)).wait_recv()
                        finish(src_z * nx + xpeer(k), p)

    for way in (1, -1):
        for step in range(nz):
            src_z = z - way * step

            @pl.when(jnp.logical_and(valid(src_z), valid(z + way)))
            def _():
                for i in range(len(items)):
                    wz(way, src_z, i, z + way).wait_send()

    for m in range(1, nx):
        for p in cross:
            wx(m, p, z, x).wait_send()
        for zi in range(nz):
            for p in direct:
                wx(m, p, zi, x).wait_send()
            dx(m, zi, x).wait_send()
        rx(m, x, xpeer(m)).wait_send()
    for k in range(1, nz):
        rz(k, z, zpeer(k)).wait_send()
        dz(k, z).wait_send()
    for k in range(1, nt):
        tp(k, t).wait_send()


def put_kernel(*refs):
    count = (len(refs) - 1) // 2
    sem = refs[-1]
    copies = [pltpu.make_async_copy(refs[i], refs[count + i], sem.at[i]) for i in range(count)]
    for copy in copies:
        copy.start()
    for copy in copies:
        copy.wait()


def per_device(nz, nx, nt, xin, gcot, fcot, scot, lam, proj, gw, gm, gs, vw, vm, vs):
    nfs = nz * nx
    rows, cg = gw.shape
    cv = vw.shape[1]
    cols = cg + cv
    depth, rank = proj.shape
    share = rank // nfs
    pieces = min(PIECES, rows // PIECE_ROWS)
    part = rows // pieces
    items = pieces + (nx - 1) * (pieces * CROSS // 8)
    dma = pltpu.SemaphoreType.DMA
    shape = jax.ShapeDtypeStruct
    vmem = lambda a: pltpu.VMEM(a.shape, a.dtype)
    results = [
        shape((rows, cg), f32),
        shape((rows, cg), f32),
        shape((depth, cg), bf16),
        shape(gm.shape, f32),
        shape(gs.shape, f32),
        shape((rows, cv), f32),
        shape((rows, cv), f32),
        shape((depth, cv), bf16),
        shape(vm.shape, f32),
        shape(vs.shape, f32),
    ]
    arrays = [xin, gcot, fcot, scot, lam, proj, gw, gm, gs, vw, vm, vs]
    alone = cv == VDIM
    arrays = [
        a if alone and a is lam else pltpu.with_memory_space_constraint(a, pltpu.HBM)
        for a in arrays
    ]
    anywhere = pl.BlockSpec(memory_space=pl.ANY)
    inside = pl.BlockSpec(memory_space=pltpu.VMEM)
    held = pl.pallas_call(
        functools.partial(kernel, nz, nx, nt),
        out_shape=[vmem(a) for a in results],
        in_specs=[
            pl.BlockSpec(memory_space=pltpu.SMEM) if alone and a is lam else anywhere
            for a in (xin, gcot, fcot, scot, lam, proj, gw, gm, gs, vw, vm, vs)
        ],
        out_specs=[inside] * 10,
        scratch_shapes=[
            pltpu.SMEM(lam.shape, lam.dtype),
            vmem(xin),
            vmem(gcot),
            vmem(fcot),
            vmem(scot),
            vmem(proj),
            vmem(gw),
            vmem(vw),
            vmem(gm),
            vmem(gs),
            vmem(vm),
            vmem(vs),
            pltpu.VMEM((nfs, pieces, part, cols), bf16),
            pltpu.VMEM((rank, cols), f32),
            pltpu.VMEM((depth, cols), f32),
            pltpu.VMEM((nx, nz, share, cols), bf16),
            pltpu.VMEM((nx, nz, share, cols), bf16),
            pltpu.VMEM((nz, share, cols), bf16),
            pltpu.VMEM((nz, share, cols), bf16),
            pltpu.VMEM((nfs, share, cols), bf16),
            pltpu.VMEM((rank, cols), f32),
            pltpu.VMEM((nt, 2, 8, 128), f32),
            dma((8,)),
            dma((4, CHUNKS)),
            dma((2, nz, items)),
            dma((nz, items)),
            dma((nx, nz, pieces)),
            dma((nx, nz, pieces)),
            dma((nx,)),
            dma((nx,)),
            dma((nz,)),
            dma((nz,)),
            dma((nz,)),
            dma((nz,)),
            dma((nx, nz)),
            dma((nx, nz)),
            dma((nt,)),
            dma((nt,)),
        ],
        compiler_params=pltpu.CompilerParams(
            collective_id=0, has_side_effects=True, vmem_limit_bytes=40 * 1024 * 1024
        ),
    )(*arrays)
    return tuple(
        pl.pallas_call(
            put_kernel,
            out_shape=results,
            in_specs=[inside] * 10,
            out_specs=[anywhere] * 10,
            scratch_shapes=[dma((10,))],
            compiler_params=pltpu.CompilerParams(vmem_limit_bytes=8 * 1024 * 1024),
        )(*held)
    )


def solution(mesh):
    nz, nx = factor_fs(mesh.shape["fs"])
    split, whole = P("fs", "tp"), P(None, "tp")
    placed = (P("fs", None), split, split, split, P("tp"), P()) + (split,) * 6
    return jax.shard_map(
        functools.partial(per_device, nz, nx, mesh.shape["tp"]),
        mesh=mesh,
        in_specs=placed,
        out_specs=(split, split, whole, split, split, split, split, whole, split, split),
        check_vma=False,
    )
```

time: 69.3 us -> 61.9 us (0.89)
  the two profiles are of different devices: /device:TPU:12 before, /device:TPU:17 now
where the time goes in v1:
time: 61.9 us; the launch traced here: 61.8 us
  Pallas kernels  61.1 us (99%)
  between operations  0.66 us (1%)
    pallas_call x1, Pallas kernels, per_device(): pl.pallas_call(functools.partial(kernel, nz, nx, nt), out_shape=[vmem(a)...  58.8 us
    pallas_call x1, Pallas kernels, per_device(): pl.pallas_call(put_kernel, out_shape=results, in_specs=[inside] * 10, out...  2.32 us

profile of v1, /device:TPU:17, one launch (start us, length us, event | category | flops | bytes accessed | tf_op | source)
XLA Modules:
  0.0 61.8 jit_solution(1843789181397773812)
XLA Ops:
  0.6 58.8 %shard_map.195 = (f32[256,512]{1,0:T(8,128)S(1)}, f32[256,512]{1,0:T(8,128)S(1)}, bf16[2048,512]{1,0:T(8,128)(2,1)S(1)}, f32[32,512]{1,0:T(8,128)S(1)}, f32[32,5...) custom-call(bf16[2048,2048]{1,0:T(8,128)(2,1)} %x_hbm.1, ...), custom_call_target="tpu_custom_call" | custom-call | tf_op jit(solution)/shard_map/pallas_call | solution.py:512
  59.4 2.3 %shard_map.196 = (f32[256,512]{1,0:T(8,128)}, f32[256,512]{1,0:T(8,128)}, bf16[2048,512]{1,0:T(8,128)(2,1)}, f32[32,512]{1,0:T(8,128)}, f32[32,512]{1,0:T(8,128)...) custom-call(f32[256,512]{1,0:T(8,128)S(1)} %get-tuple-element.20.ref, ...), custom_call_target="tpu_custom_call" | custom-call | tf_op jit(solution)/shard_map/pallas_call | solution.py:565

commit v2 on v1

--- a/solution.py
+++ b/solution.py
@@ -10,13 +10,15 @@
 VDIM = 128
 PIECES = 8
 PIECE_ROWS = 16
-CROSS = 1
+CROSS_END = 1
+CROSS_INNER = 2
 CHUNKS = 4
-STEP_TOKENS = 256
-HOLD_X = 4
-HOLD_ONE = 6
-HOLD_TWO = 4
-HOLD_THREE = 4
+DEPTH = 3
+HOLD_X = 5
+R1A = 2
+R1B = 5
+R2A = 4
+R3A = 2
 
 moment_decay = 0.9
 square_decay = 0.95
@@ -74,6 +76,7 @@
     vm,
     vs,
     wall,
+    proj_t,
     acc,
     updates,
     rsrc,
@@ -112,9 +115,9 @@
     share = rank // nfs
     pieces, part = wall.shape[1:3]
     tokens = x_hbm.shape[0] // CHUNKS
-    cross = range(pieces * CROSS // 8)
-    direct = range(len(cross), pieces)
-    items = [(0, p) for p in range(pieces)] + [(k, p) for p in cross for k in range(1, nx)]
+    cross_end = pieces * CROSS_END // PIECES
+    cross_inner = pieces * CROSS_INNER // PIECES
+    items = [(k, p) for k in range(nx) for p in range(pieces)]
 
     def zpeer(k):
         return lax.rem(z + k, nz)
@@ -158,16 +161,13 @@
             )
         ]
 
-    for copy in small[:3] + small[7:]:
+    for copy in small[:3] + small[7:] + chunk_copies(0):
         copy.start()
-    for c in range(CHUNKS):
+    small[0].wait()
+    small[1].wait()
+    for c in range(1, DEPTH):
         for copy in chunk_copies(c):
             copy.start()
-    for i in range(3, 7):
-        small[i].start()
-
-    small[0].wait()
-    small[1].wait()
     for p in range(pieces):
         at = pl.ds(p * part, part)
         wall[f, p, :, :cg] = gw[at, :].astype(bf16)
@@ -176,14 +176,19 @@
     def valid(row):
         return jnp.logical_and(row >= 0, row < nz)
 
-    def wz(way, src_z, i, peer):
-        k, p = items[i]
+    def at_end(row):
+        return jnp.logical_or(row == 0, row == nz - 1)
+
+    def crosses(p, row):
+        return jnp.logical_or(p < cross_end, jnp.logical_and(p < cross_inner, jnp.logical_not(at_end(row))))
+
+    def wz(way, src_z, k, p, peer):
         owner = src_z * nx + xpeer(k)
         return pltpu.make_async_remote_copy(
             src_ref=wall.at[owner, p],
             dst_ref=wall.at[owner, p],
-            send_sem=wz_send.at[(way + 1) // 2, src_z, i],
-            recv_sem=wz_recv.at[src_z, i],
+            send_sem=wz_send.at[(way + 1) // 2, src_z, k],
+            recv_sem=wz_recv.at[src_z, k, p] if isinstance(p, int) else wz_recv.at[src_z, k, 0],
             device_id=(peer * nx + x, t),
             device_id_type=MESH,
         )
@@ -193,52 +198,102 @@
         return pltpu.make_async_remote_copy(
             src_ref=wall.at[owner, p],
             dst_ref=wall.at[owner, p],
-            send_sem=wx_send.at[k, src_z, p],
-            recv_sem=wx_recv.at[src_x, src_z, p],
+            send_sem=wx_send.at[k, src_z],
+            recv_sem=wx_recv.at[src_x, src_z, p] if isinstance(p, int) else wx_recv.at[src_x, src_z, 0],
             device_id=(z * nx + xpeer(k), t),
             device_id_type=MESH,
         )
 
-    def along(way, src_z, i):
-        @pl.when(valid(z + way))
-        def _():
-            wz(way, src_z, i, z + way).start()
+    def along(src_z, k, p):
+        for way in (1, -1):
+
+            @pl.when(valid(z + way))
+            def _():
+                wz(way, src_z, k, p, z + way).start()
 
     def over(src_z, p):
         for k in range(1, nx):
             wx(k, p, src_z, x).start()
 
-    def relay(step, i):
-        k, p = items[i]
+    def rides(step, p, src_z):
+        here = crosses(p, src_z)
+        return jnp.logical_or(here, at_end(src_z)) if step < 2 else here
+
+    def relay(step, k, p):
         for way in (1, -1):
             src_z = z - way * step
 
-            @pl.when(valid(src_z))
+            @pl.when(jnp.logical_and(valid(src_z), rides(step, p, src_z) if k else True))
             def _():
-                wz(way, src_z, i, z - way).wait_recv()
-                along(way, src_z, i)
-                if k == 0 and p in direct:
-                    over(src_z, p)
-
-    def cross_over():
-        for i in range(pieces, len(items)):
-            k, p = items[i]
-            wx(k, p, z, xpeer(k)).wait_recv()
-            for way in (1, -1):
-                along(way, z, i)
+                wz(way, src_z, k, p, z - way).wait_recv()
+
+                @pl.when(jnp.logical_and(valid(z + way), crosses(p, src_z) if k else True))
+                def _():
+                    wz(way, src_z, k, p, z + way).start()
+
+                if not k:
+
+                    @pl.when(jnp.logical_not(rides(step, p, src_z)))
+                    def _():
+                        over(src_z, p)
+
+    def relays(step, others, lo, hi):
+        if step < nz:
+            for p in range(min(lo, pieces), min(hi, pieces)):
+                for k in range(1, nx) if others else (0,):
+                    relay(step, k, p)
+
+    def turns(lo, hi):
+        for p in range(min(lo, pieces), min(hi, pieces)):
+            for k in range(1, nx):
+                wx(k, p, z, xpeer(k)).wait_recv()
+
+                @pl.when(rides(0, p, z))
+                def _():
+                    along(z, k, p)
+
+    def sent(step):
+        for way in (1, -1) if step else (0,):
+            src_z = z - way * step
+            end = at_end(src_z)
+            for go in (way,) if step else (1, -1):
+                onward = jnp.logical_and(valid(src_z), valid(z + go))
+
+                @pl.when(onward)
+                def _():
+                    wz(go, src_z, 0, pl.ds(0, pieces), z + go).wait_send()
+
+                for count, case in (
+                    (cross_end if step else pieces, end),
+                    (cross_inner, jnp.logical_not(end)),
+                ):
+                    if count:
+
+                        @pl.when(jnp.logical_and(onward, case))
+                        def _():
+                            for k in range(1, nx):
+                                wz(go, src_z, k, pl.ds(0, count), z + go).wait_send()
+
+            for first, case in ((cross_end, end), (cross_inner, jnp.logical_not(end))):
+                if step == 1 and first == cross_end and case is end:
+                    continue
+                if not step:
+                    first = 0
+
+                @pl.when(jnp.logical_and(valid(src_z), case))
+                def _():
+                    for k in range(1, nx):
+                        wx(k, pl.ds(first, pieces - first), src_z, x).wait_send()
 
     pl.semaphore_wait(barrier, (nz - 1) + (nx - 1) + (nt - 1))
-    for p in cross:
-        over(z, p)
     for p in range(pieces):
-        for way in (1, -1):
-            along(way, z, p)
-        if p in direct and p < HOLD_X:
+        along(z, 0, p)
+        if p < HOLD_X:
             over(z, p)
 
     for copy in small[2:3] + small[7:]:
         copy.wait()
-    acc[...] = jnp.zeros_like(acc)
+    proj_t[...] = pv[...].T
     head = lax.broadcasted_iota(jnp.int32, (1, cv), 1) // VDIM
     lam = jnp.zeros((1, cv), f32)
     for h in range(cv // VDIM):
@@ -247,53 +302,39 @@
         for copy in chunk_copies(c):
             copy.wait()
 
-        def multiply(i, carry):
-            at = pl.ds(pl.multiple_of(c * tokens + i * STEP_TOKENS, STEP_TOKENS), STEP_TOKENS)
-            upper = jnp.dot(xv[at, :], pv[...], preferred_element_type=f32).astype(bf16)
-            value = (fcv[at, :].astype(f32) - lam * scv[at, :].astype(f32)).astype(bf16)
-            across = (((0,), (0,)), ((), ()))
-            acc[:, :cg] += lax.dot_general(upper, gcv[at, :], across, preferred_element_type=f32)
-            acc[:, cg:] += lax.dot_general(upper, value, across, preferred_element_type=f32)
-            return carry
-
-        lax.fori_loop(0, tokens // STEP_TOKENS, multiply, 0)
+        if c + DEPTH < CHUNKS:
+            for copy in chunk_copies(c + DEPTH):
+                copy.start()
+        elif c + DEPTH == CHUNKS:
+            for i in range(3, 7):
+                small[i].start()
+        at = pl.ds(c * tokens, tokens)
+        upper = lax.dot_general(
+            proj_t[...], xv[at, :], (((1,), (1,)), ((), ())), preferred_element_type=f32
+        ).astype(bf16)
+        value = (fcv[at, :].astype(f32) - lam * scv[at, :].astype(f32)).astype(bf16)
+        gate_part = jnp.dot(upper, gcv[at, :], preferred_element_type=f32)
+        value_part = jnp.dot(upper, value, preferred_element_type=f32)
+        if c:
+            gate_part += acc[:, :cg]
+            value_part += acc[:, cg:]
+        acc[:, :cg] = gate_part
+        acc[:, cg:] = value_part
 
     for zi in range(nz):
         for xi in range(nx):
             at = pl.ds((zi * nx + xi) * share, share)
             rsrc[xi, zi] = acc[at, :].astype(bf16)
 
-    def rx(k, src_x, dst_x):
+    def rx(k, zi, src_x, dst_x):
         return pltpu.make_async_remote_copy(
-            src_ref=rsrc.at[dst_x],
-            dst_ref=rsx.at[src_x],
-            send_sem=rx_send.at[k],
-            recv_sem=rx_recv.at[src_x],
+            src_ref=rsrc.at[dst_x, zi],
+            dst_ref=rsx.at[src_x, zi],
+            send_sem=rx_send.at[k, zi],
+            recv_sem=rx_recv.at[src_x, zi],
             device_id=(z * nx + xpeer(k), t),
             device_id_type=MESH,
         )
-
-    for k in range(1, nx):
-        rx(k, x, xpeer(k)).start()
-    cross_over()
-    for p in direct:
-        if p >= HOLD_X:
-            over(z, p)
-
-    def relays(step, lo, hi):
-        if step < nz:
-            for i in range(min(lo, len(items)), min(hi, len(items))):
-                relay(step, i)
-
-    relays(1, 0, HOLD_ONE)
-    for k in range(1, nx):
-        rx(k, xpeer(k), x).wait_recv()
-    for zi in range(nz):
-        at = pl.ds(pl.multiple_of((zi * nx + x) * share, share), share)
-        total = acc[at, :]
-        for k in range(1, nx):
-            total = total + rsx[xpeer(k), zi].astype(f32)
-        zsrc[zi] = total.astype(bf16)
 
     def rz(k, src_z, dst_z):
         return pltpu.make_async_remote_copy(
@@ -305,13 +346,30 @@
             device_id_type=MESH,
         )
 
-    for k in range(1, nz):
-        rz(k, z, zpeer(k)).start()
-    relays(1, HOLD_ONE, len(items))
-    relays(2, 0, HOLD_TWO)
+    def column_sum(zi):
+        at = pl.ds(pl.multiple_of((zi * nx + x) * share, share), share)
+        total = acc[at, :]
+        for k in range(1, nx):
+            rx(k, zi, xpeer(k), x).wait_recv()
+            total = total + rsx[xpeer(k), zi].astype(f32)
+        return total
+
+    far = list(range(1, nz))
+    for j in far + [0]:
+        for k in range(1, nx):
+            rx(k, zpeer(j), x, xpeer(k)).start()
+    for p in range(min(HOLD_X, pieces), pieces):
+        over(z, p)
+    relays(1, 0, 0, R1A)
+    turns(0, R1A)
+    for j in far:
+        zsrc[zpeer(j)] = column_sum(zpeer(j)).astype(bf16)
+        rz(j, z, zpeer(j)).start()
+    relays(1, 0, R1A, R1B)
+    turns(R1A, R1B)
     for i in range(3, 7):
         small[i].wait()
-    low = zsrc[z].astype(f32)
+    low = column_sum(z)
     for k in range(1, nz):
         rz(k, zpeer(k), z).wait_recv()
         low = low + rsz[zpeer(k)].astype(f32)
@@ -353,12 +411,17 @@
         dz(k, z).start()
     for m in range(1, nx):
         dx(m, z, x).start()
-    relays(2, HOLD_TWO, len(items))
+    relays(1, 0, R1B, pieces)
+    turns(R1B, pieces)
+    relays(1, 1, 0, cross_inner)
+    relays(2, 0, 0, R2A)
     for k in range(1, nz):
         dz(k, zpeer(k)).wait_recv()
         for m in range(1, nx):
             dx(m, zpeer(k), x).start()
-    relays(3, 0, HOLD_THREE)
+    relays(2, 0, R2A, pieces)
+    relays(2, 1, 0, cross_inner)
+    relays(3, 0, 0, R3A)
     for m in range(1, nx):
         for zi in range(nz):
             dx(m, zi, xpeer(m)).wait_recv()
@@ -392,9 +455,12 @@
 
     for k in range(1, nt):
         tp(k, t).start()
-    relays(3, HOLD_THREE, len(items))
+    relays(3, 0, R3A, pieces)
+    relays(3, 1, 0, cross_inner)
     for step in range(4, nz):
-        relays(step, 0, len(items))
+        relays(step, 0, 0, pieces)
+        relays(step, 1, 0, cross_inner)
+    relays(1, 1, cross_inner, pieces)
     for k in range(1, nt):
         tp(k, lax.rem(t + k, nt)).wait_recv()
     whole = sums[0]
@@ -428,42 +494,38 @@
 
     for zi in range(nz):
         finish_block(zi * nx + x, 0, pieces)
-        if len(cross):
-            for k in range(1, nx):
-                finish_block(zi * nx + xpeer(k), 0, len(cross))
-    for step in range(nz):
-        for p in direct:
-            for way in (1, -1) if step else (1,):
+        for k in range(1, nx):
+            finish_block(zi * nx + xpeer(k), 0, cross_end)
+    for k in range(1, nx):
+        finish_block(z * nx + xpeer(k), cross_end, pieces)
+    for k in range(1, nz):
+        rz(k, z, zpeer(k)).wait_send()
+        dz(k, z).wait_send()
+    for m in range(1, nx):
+        for zi in range(nz):
+            dx(m, zi, x).wait_send()
+            rx(m, zi, x, xpeer(m)).wait_send()
+    for k in range(1, nt):
+        tp(k, t).wait_send()
+    for step in range(max(nz - 1, 1)):
+        sent(step)
+    for step in range(1, nz):
+        for p in range(cross_end, pieces):
+            for way in (1, -1):
                 src_z = z - way * step
 
                 @pl.when(valid(src_z))
                 def _():
                     for k in range(1, nx):
-                        wx(k, p, src_z, xpeer(k)).wait_recv()
+
+                        @pl.when(jnp.logical_not(rides(step, p, src_z)))
+                        def _():
+                            wx(k, p, src_z, xpeer(k)).wait_recv()
+
                         finish(src_z * nx + xpeer(k), p)
 
-    for way in (1, -1):
-        for step in range(nz):
-            src_z = z - way * step
-
-            @pl.when(jnp.logical_and(valid(src_z), valid(z + way)))
-            def _():
-                for i in range(len(items)):
-                    wz(way, src_z, i, z + way).wait_send()
-
-    for m in range(1, nx):
-        for p in cross:
-            wx(m, p, z, x).wait_send()
-        for zi in range(nz):
-            for p in direct:
-                wx(m, p, zi, x).wait_send()
-            dx(m, zi, x).wait_send()
-        rx(m, x, xpeer(m)).wait_send()
-    for k in range(1, nz):
-        rz(k, z, zpeer(k)).wait_send()
-        dz(k, z).wait_send()
-    for k in range(1, nt):
-        tp(k, t).wait_send()
+    if nz > 1:
+        sent(nz - 1)
 
 
 def put_kernel(*refs):
@@ -485,7 +547,6 @@
     share = rank // nfs
     pieces = min(PIECES, rows // PIECE_ROWS)
     part = rows // pieces
-    items = pieces + (nx - 1) * (pieces * CROSS // 8)
     dma = pltpu.SemaphoreType.DMA
     shape = jax.ShapeDtypeStruct
     vmem = lambda a: pltpu.VMEM(a.shape, a.dtype)
@@ -531,6 +592,7 @@
             vmem(vm),
             vmem(vs),
             pltpu.VMEM((nfs, pieces, part, cols), bf16),
+            pltpu.VMEM((rank, depth), bf16),
             pltpu.VMEM((rank, cols), f32),
             pltpu.VMEM((depth, cols), f32),
             pltpu.VMEM((nx, nz, share, cols), bf16),
@@ -542,12 +604,12 @@
             pltpu.VMEM((nt, 2, 8, 128), f32),
             dma((8,)),
             dma((4, CHUNKS)),
-            dma((2, nz, items)),
-            dma((nz, items)),
+            dma((2, nz, nx)),
+            dma((nz, nx, pieces)),
+            dma((nx, nz)),
             dma((nx, nz, pieces)),
-            dma((nx, nz, pieces)),
-            dma((nx,)),
-            dma((nx,)),
+            dma((nx, nz)),
+            dma((nx, nz)),
             dma((nz,)),
             dma((nz,)),
             dma((nz,)),

time: 61.9 us -> 51.5 us (0.83)
  the two profiles are of different devices: /device:TPU:17 before, /device:TPU:0 now
where the time goes in v2:
time: 51.5 us; the launch traced here: 51.4 us
  Pallas kernels  50.7 us (98%)
  between operations  0.66 us (1%)
    pallas_call x1, Pallas kernels, per_device(): pl.pallas_call(functools.partial(kernel, nz, nx, nt), out_shape=[vmem(a)...  48.4 us
    pallas_call x1, Pallas kernels, per_device(): pl.pallas_call(put_kernel, out_shape=results, in_specs=[inside] * 10, out...  2.32 us

profile of v2, /device:TPU:0, one launch (start us, length us, event | category | flops | bytes accessed | tf_op | source)
XLA Modules:
  0.0 51.4 jit_solution(2399397671494453445)
XLA Ops:
  0.6 48.4 %shard_map.195 = (f32[256,512]{1,0:T(8,128)S(1)}, f32[256,512]{1,0:T(8,128)S(1)}, bf16[2048,512]{1,0:T(8,128)(2,1)S(1)}, f32[32,512]{1,0:T(8,128)S(1)}, f32[32,5...) custom-call(bf16[2048,2048]{1,0:T(8,128)(2,1)} %x_hbm.1, ...), custom_call_target="tpu_custom_call" | custom-call | tf_op jit(solution)/shard_map/pallas_call | solution.py:573
  49.1 2.3 %shard_map.196 = (f32[256,512]{1,0:T(8,128)}, f32[256,512]{1,0:T(8,128)}, bf16[2048,512]{1,0:T(8,128)(2,1)}, f32[32,512]{1,0:T(8,128)}, f32[32,512]{1,0:T(8,128)...) custom-call(f32[256,512]{1,0:T(8,128)S(1)} %get-tuple-element.20.ref, ...), custom_call_target="tpu_custom_call" | custom-call | tf_op jit(solution)/shard_map/pallas_call | solution.py:627

commit v3 on v2

v3 whole, which is shorter than its diff:
```python
import functools

import jax
import jax.numpy as jnp
from jax import lax
from jax.experimental import pallas as pl
from jax.experimental.pallas import tpu as pltpu
from jax.sharding import PartitionSpec as P

VDIM = 128
PIECES = 8
PIECE_ROWS = 16
CROSS_END = 1
CROSS_INNER = 1
CHUNKS = 4
DEPTH = 3
SINGLES = 2
HOLD_X = 5
HOLD_Z = 5
FIRST_A = (0, 5, 0, 4)
FIRST_B = (5, 8, 4, 6)
FIRST_C = (8, 8, 6, 8)
SECOND_A = (0, 7, 0, 3)
SECOND_B = (7, 8, 3, 8)
THIRD_A = (0, 4, 0, 4)
THIRD_B = (4, 6, 4, 6)
THIRD_C = (6, 8, 6, 8)

moment_decay = 0.9
square_decay = 0.95
adam_floor = 1e-08
learn_rate = 0.02
rms_floor = 0.1

MESH = pl.DeviceIdType.MESH
f32, bf16 = jnp.float32, jnp.bfloat16


def factor_fs(count):
    inner = 1
    while (2 * inner) ** 2 <= count and count % (2 * inner) == 0:
        inner *= 2
    return count // inner, inner


def kernel(
    nz,
    nx,
    nt,
    x_hbm,
    gcot_hbm,
    fcot_hbm,
    scot_hbm,
    lam_hbm,
    proj_hbm,
    gw_hbm,
    gm_hbm,
    gs_hbm,
    vw_hbm,
    vm_hbm,
    vs_hbm,
    new_gw,
    gsteps,
    gcopy,
    new_gm,
    new_gs,
    new_vw,
    vsteps,
    vcopy,
    new_vm,
    new_vs,
    lam_ref,
    xv,
    gcv,
    fcv,
    scv,
    pv,
    gw,
    vw,
    gm,
    gs,
    vm,
    vs,
    wall,
    proj_t,
    gram_high,
    gram_low,
    acc,
    updates,
    rsrc,
    rsx,
    zsrc,
    rsz,
    handed,
    low,
    dall,
    dcat,
    sums,
    in_sem,
    x_sem,
    wz_send,
    wz_recv,
    wz_more,
    wx_send,
    wx_recv,
    wx_own,
    rx_send,
    rx_recv,
    rz_send,
    rz_recv,
    dz_send,
    dz_recv,
    dx_send,
    dx_recv,
    t_send,
    t_recv,
    far_sem,
    hand_send,
    hand_recv,
):
    nfs = nz * nx
    f = lax.axis_index("fs")
    t = lax.axis_index("tp")
    z = lax.div(f, nx)
    x = lax.rem(f, nx)
    rows, cg = gw.shape
    cv = vw.shape[1]
    cols = cg + cv
    rank = acc.shape[0]
    share = rank // nfs
    part = wall.shape[1]
    pieces = rows // part
    tokens = x_hbm.shape[0] // CHUNKS
    cross_end = pieces * CROSS_END // PIECES
    cross_inner = pieces * CROSS_INNER // PIECES
    items = [(k, p) for k in range(nx) for p in range(pieces)]

    def zpeer(k):
        return lax.rem(z + k, nz)

    def xpeer(k):
        return lax.rem(x + k, nx)

    def valid(row):
        return jnp.logical_and(row >= 0, row < nz)

    barrier = pltpu.get_barrier_semaphore()
    for way in (1, -1):

        @pl.when(valid(z + way))
        def _():
            pl.semaphore_signal(barrier, inc=1, device_id=((z + way) * nx + x, t), device_id_type=MESH)

    for k in range(1, nx):
        pl.semaphore_signal(barrier, inc=1, device_id=(z * nx + xpeer(k), t), device_id_type=MESH)
    for k in range(1, nt):
        pl.semaphore_signal(barrier, inc=1, device_id=(f, lax.rem(t + k, nt)), device_id_type=MESH)

    small = [
        pltpu.make_async_copy(src, dst, in_sem.at[i])
        for i, (src, dst) in enumerate(
            [
                (gw_hbm, gw),
                (vw_hbm, vw),
                (proj_hbm, pv),
                (gm_hbm, gm),
                (gs_hbm, gs),
                (vm_hbm, vm),
                (vs_hbm, vs),
                (lam_hbm, lam_ref),
            ]
        )
        if src is not lam_hbm or cv > VDIM
    ]
    if cv == VDIM:
        lam_ref = lam_hbm

    def chunk_copies(c):
        at = pl.ds(c * tokens, tokens)
        return [
            pltpu.make_async_copy(src.at[at], dst.at[at], x_sem.at[i, c % DEPTH])
            for i, (src, dst) in enumerate(
                [(x_hbm, xv), (gcot_hbm, gcv), (fcot_hbm, fcv), (scot_hbm, scv)]
            )
        ]

    for copy in small[:3] + small[7:] + chunk_copies(0):
        copy.start()
    small[0].wait()
    small[1].wait()
    for c in range(1, DEPTH):
        for copy in chunk_copies(c):
            copy.start()
    for p in range(pieces):
        at = pl.ds(p * part, part)
        wall[f * pieces + p, :, :cg] = gw[at, :].astype(bf16)
        wall[f * pieces + p, :, cg:] = vw[at, :].astype(bf16)

    def at_end(row):
        return jnp.logical_or(row == 0, row == nz - 1)

    def crosses(p, row):
        return jnp.logical_or(p < cross_end, jnp.logical_and(p < cross_inner, jnp.logical_not(at_end(row))))

    def wz(way, src_z, k, p, peer, here=False):
        at = (src_z * nx + xpeer(k)) * pieces + p
        away = lax.rem(src_z - (z if here else peer) + nz, nz) - 1
        if k and p >= cross_inner:
            sem = wz_recv.at[away, pieces]
        elif k:
            sem = wz_more.at[away, (k - 1) * max(cross_inner, 1) + p]
        else:
            sem = wz_recv.at[away, p]
        return pltpu.make_async_remote_copy(
            src_ref=wall.at[at],
            dst_ref=wall.at[at],
            send_sem=wz_send.at[(way + 1) // 2, src_z],
            recv_sem=sem,
            device_id=(peer * nx + x, t),
            device_id_type=MESH,
        )

    def wx(k, p, src_z, src_x, own):
        at = (src_z * nx + src_x) * pieces + p
        if own:
            sem = wx_own.at[nx - k - 1, p]
        else:
            sem = wx_recv.at[nx - k - 1, lax.rem(src_z - z + nz, nz) - 1, group_of(p)]
        return pltpu.make_async_remote_copy(
            src_ref=wall.at[at],
            dst_ref=wall.at[at],
            send_sem=wx_send.at[k - 1, src_z],
            recv_sem=sem,
            device_id=(z * nx + xpeer(k), t),
            device_id_type=MESH,
        )

    def group_of(p):
        return max(p - (pieces - SINGLES) + 1, 0)

    def await_sent(sem, count):
        pieces_of = wall.at[pl.ds(0, count)]
        pltpu.make_async_remote_copy(
            src_ref=pieces_of,
            dst_ref=pieces_of,
            send_sem=sem,
            recv_sem=sem,
            device_id=(z * nx + xpeer(1), t),
            device_id_type=MESH,
        ).wait_send()

    def await_got(sem, ref):
        pltpu.make_async_remote_copy(
            src_ref=ref,
            dst_ref=ref,
            send_sem=sem,
            recv_sem=sem,
            device_id=(z * nx + xpeer(1), t),
            device_id_type=MESH,
        ).wait_recv()

    def along(src_z, k, p):
        for way in (1, -1):

            @pl.when(valid(z + way))
            def _():
                wz(way, src_z, k, p, z + way).start()

    def over(src_z, p, own=False):
        for k in range(1, nx):
            wx(k, p, src_z, x, own).start()

    def rides(step, p, src_z):
        here = crosses(p, src_z)
        return jnp.logical_or(here, at_end(src_z)) if step < 2 else here

    def relay(step, k, p, where):
        for way in (1, -1):
            src_z = z - way * step
            come = jnp.logical_and(valid(src_z), where)
            if k:
                come = jnp.logical_and(come, crosses(p, src_z))

            @pl.when(come)
            def _():
                wz(way, src_z, k, p, z - way, True).wait_recv()

                @pl.when(valid(z + way))
                def _():
                    wz(way, src_z, k, p, z + way).start()

                if not k:

                    @pl.when(jnp.logical_not(rides(step, p, src_z)))
                    def _():
                        over(src_z, p)

    def relays(step, lo_end, hi_end, lo, hi):
        if step < nz:
            for p in range(pieces):
                ends, rest = lo_end <= p < hi_end, lo <= p < hi
                if ends or rest:
                    where = True if ends and rest else end if ends else jnp.logical_not(end)
                    relay(step, 0, p, where)

    def relay_others(step, where):
        if step < nz:
            for p in range(cross_inner):
                for k in range(1, nx):
                    relay(step, k, p, where)

    def turns(lo, hi):
        for p in range(min(lo, pieces), min(hi, pieces)):
            for k in range(1, nx):
                await_got(wx_own.at[k - 1, p], wall.at[p])

                @pl.when(rides(0, p, z))
                def _():
                    along(z, k, p)

    def sent(step):
        for way in (1, -1) if step else (0,):
            src_z = z - way * step
            src_end = at_end(src_z)
            for case, many, crossing, passed in (
                (src_end, cross_end if step else pieces, cross_end, step == 1),
                (jnp.logical_not(src_end), cross_inner, cross_inner, False),
            ):

                @pl.when(jnp.logical_and(valid(src_z), case))
                def _():
                    for go in (way,) if step else (1, -1):

                        @pl.when(valid(z + go))
                        def _():
                            await_sent(wz_send.at[(go + 1) // 2, src_z], pieces + (nx - 1) * many)

                    if not passed:
                        for k in range(1, nx):
                            await_sent(wx_send.at[k - 1, src_z], pieces - crossing if step else pieces)

    end = at_end(z)
    next_rows = jnp.where(valid(z + 1), 1, 0) + jnp.where(valid(z - 1), 1, 0)

    def tell(i):
        if i < nz - 2:
            for way in (1, -1):

                @pl.when(valid(z + way))
                def _():
                    pl.semaphore_signal(
                        far_sem.at[i], inc=1, device_id=((z + way) * nx + x, t), device_id_type=MESH
                    )

    def hear(i):
        if i < nz - 2:
            pl.semaphore_wait(far_sem.at[i], next_rows)

    pl.semaphore_wait(barrier, next_rows + (nx - 1) + (nt - 1))
    tell(0)
    for p in range(pieces):
        if p < HOLD_Z:
            along(z, 0, p)
        else:

            @pl.when(jnp.logical_not(end))
            def _():
                along(z, 0, p)

        if p < HOLD_X:
            over(z, p, True)

    for copy in small[2:3] + small[7:]:
        copy.wait()
    proj_t[...] = pv[...].T
    head = lax.broadcasted_iota(jnp.int32, (1, cv), 1) // VDIM
    lam = jnp.zeros((1, cv), f32)
    for h in range(cv // VDIM):
        lam = jnp.where(head == h, lam_ref[h], lam)
    for c in range(CHUNKS):
        for copy in chunk_copies(c):
            copy.wait()

        if c + DEPTH < CHUNKS:
            for copy in chunk_copies(c + DEPTH):
                copy.start()
        elif c + DEPTH == CHUNKS:
            for i in range(3, 7):
                small[i].start()
        at = pl.ds(c * tokens, tokens)
        upper = lax.dot_general(
            proj_t[...], xv[at, :], (((1,), (1,)), ((), ())), preferred_element_type=f32
        ).astype(bf16)
        value = (fcv[at, :].astype(f32) - lam * scv[at, :].astype(f32)).astype(bf16)
        gate_part = jnp.dot(upper, gcv[at, :], preferred_element_type=f32)
        value_part = jnp.dot(upper, value, preferred_element_type=f32)
        if c:
            gate_part += acc[:, :cg]
            value_part += acc[:, cg:]
        acc[:, :cg] = gate_part
        acc[:, cg:] = value_part
        if c % 2:
            hear(c // 2)
            tell(c // 2 + 1)

    for i in range(CHUNKS // 2, nz - 2):
        hear(i)
        tell(i + 1)
    for zi in range(nz):
        for xi in range(nx):
            at = pl.ds((zi * nx + xi) * share, share)
            rsrc[xi, zi] = acc[at, :].astype(bf16)

    def rx(k, zi):
        return pltpu.make_async_remote_copy(
            src_ref=rsrc.at[xpeer(k), zi],
            dst_ref=rsx.at[nx - k - 1, zi],
            send_sem=rx_send.at[k - 1],
            recv_sem=rx_recv.at[nx - k - 1, zi],
            device_id=(z * nx + xpeer(k), t),
            device_id_type=MESH,
        )

    def hand(k, zi):
        row = jnp.where(z == 0, 1, nz - 2)
        return pltpu.make_async_remote_copy(
            src_ref=rsrc.at[xpeer(k), zi],
            dst_ref=handed.at[zi, (nx - k) % nx],
            send_sem=hand_send.at[0],
            recv_sem=hand_recv.at[zi],
            device_id=(row * nx + xpeer(k), t),
            device_id_type=MESH,
        )

    def rz(zi):
        return pltpu.make_async_remote_copy(
            src_ref=zsrc.at[zi],
            dst_ref=rsz.at[z - 1],
            send_sem=rz_send.at[0],
            recv_sem=rz_recv.at[0],
            device_id=(zi * nx + x, t),
            device_id_type=MESH,
        )

    far = list(range(1, nz))

    def other(j):
        return jnp.where(2 * z < nz, lax.rem(z + nz - j, nz), zpeer(j))

    def handing(j):
        return jnp.where(z == 0, nz - j, j - 1)

    inner = jnp.logical_not(end)
    beside = jnp.logical_or(z == 1, z == nz - 2)

    def row_sum(zi):
        at = pl.ds(pl.multiple_of((zi * nx + x) * share, share), share)
        low[...] = acc[at, :]
        for k in range(1, nx):
            await_got(rx_recv.at[k - 1, zi], rsx.at[0, 0])
            low[...] += rsx[k - 1, zi].astype(f32)

        @pl.when(jnp.logical_and(beside, zi != jnp.where(z == 1, 0, nz - 1)))
        def _():
            await_got(hand_recv.at[zi], handed.at[0])
            for k in range(nx):
                low[...] += handed[zi, k].astype(f32)

    @pl.when(inner)
    def _():
        for j in far:
            for k in range(1, nx):
                rx(k, other(j)).start()

    @pl.when(end)
    def _():
        for j in far:
            for k in list(range(1, nx)) + [0]:
                hand(k, handing(j)).start()

    for k in range(1, nx):
        rx(k, z).start()

    def rest_over():
        for p in range(min(HOLD_X, pieces), pieces):
            over(z, p, True)

    pl.when(end)(rest_over)

    @pl.when(end)
    def _():
        for p in range(min(HOLD_Z, pieces), pieces):
            along(z, 0, p)

    relays(1, *FIRST_A)
    gram = jnp.dot(proj_t[...], pv[...], preferred_element_type=f32)
    gram_high[...] = gram.astype(bf16)
    gram_low[...] = (gram - gram_high[...].astype(f32)).astype(bf16)

    @pl.when(inner)
    def _():
        for j in far:
            row_sum(other(j))
            zsrc[other(j)] = low[...].astype(bf16)
            rz(other(j)).start()

    pl.when(inner)(rest_over)
    relays(1, *FIRST_B)
    for i in range(3, 7):
        small[i].wait()
    row_sum(z)

    @pl.when(end)
    def _():
        await_got(rz_recv.at[0], rsz.at[pl.ds(0, nz - 2)])

    @pl.when(inner)
    def _():
        await_got(rz_recv.at[0], rsz.at[pl.ds(0, nz - 3)])

    for row in range(1, nz - 1):

        @pl.when(z != row)
        def _():
            low[...] += rsz[row - 1].astype(f32)

    for first, second, new_m, new_s, at in (
        (gm, gs, new_gm, new_gs, slice(0, cg)),
        (vm, vs, new_vm, new_vs, slice(cg, cols)),
    ):
        mine = low[:, at]
        new_first = moment_decay * first[...] + (1.0 - moment_decay) * mine
        new_second = square_decay * second[...] + (1.0 - square_decay) * mine * mine
        new_m[...] = new_first
        new_s[...] = new_second
        dall[f, :, at] = (new_first / (jnp.sqrt(new_second) + adam_floor)).astype(bf16)

    def dz(k, src_z):
        owner = src_z * nx + x
        return pltpu.make_async_remote_copy(
            src_ref=dall.at[owner],
            dst_ref=dall.at[owner],
            send_sem=dz_send.at[0],
            recv_sem=dz_recv.at[src_z],
            device_id=(zpeer(k) * nx + x, t),
            device_id_type=MESH,
        )

    def dx(k, src_z, src_x):
        owner = src_z * nx + src_x
        return pltpu.make_async_remote_copy(
            src_ref=dall.at[owner],
            dst_ref=dall.at[owner],
            send_sem=dx_send.at[k - 1],
            recv_sem=dx_recv.at[nx - k - 1],
            device_id=(z * nx + xpeer(k), t),
            device_id_type=MESH,
        )

    for k in range(1, nz):
        dz(k, z).start()
    for m in range(1, nx):
        dx(m, z, x).start()
    relays(1, *FIRST_C)
    turns(0, HOLD_X)
    relays(2, *SECOND_A)
    for k in range(1, nz):
        dz(k, zpeer(k)).wait_recv()
        for m in range(1, nx):
            dx(m, zpeer(k), x).start()
    relays(2, *SECOND_B)
    turns(HOLD_X, pieces)
    relay_others(1, jnp.logical_not(end))
    relays(3, *THIRD_A)
    for m in range(1, nx):
        await_got(dx_recv.at[m - 1], dall.at[pl.ds(0, nz)])

    for j in range(nfs):
        dcat[pl.ds(j * share, share), :] = dall[j].astype(f32)
    direction = dcat[...].astype(bf16)

    turned = jnp.dot(gram_high[...], direction, preferred_element_type=f32)
    turned += jnp.dot(gram_low[...], direction, preferred_element_type=f32)
    squares = jnp.sum((turned * dcat[...]).reshape(rank // 8, 8, cols), axis=0)
    squares = jnp.sum(squares, axis=0, keepdims=True)
    squares = jnp.maximum(squares, 0.0)
    gate_sum = jnp.sum(squares[:, :cg], axis=1, keepdims=True)
    value_sum = jnp.sum(squares[:, cg:], axis=1, keepdims=True)
    sums[t, 0] = jnp.broadcast_to(gate_sum, (8, 128))
    sums[t, 1] = jnp.broadcast_to(value_sum, (8, 128))

    def tp(k, src_t):
        return pltpu.make_async_remote_copy(
            src_ref=sums.at[src_t],
            dst_ref=sums.at[src_t],
            send_sem=t_send.at[0],
            recv_sem=t_recv.at[0],
            device_id=(f, lax.rem(t + k, nt)),
            device_id_type=MESH,
        )

    for k in range(1, nt):
        tp(k, t).start()

    def expand(j, carry):
        at = pl.ds(pl.multiple_of(j * rows, rows), rows)
        updates[at, :] = jnp.dot(pv[at, :], direction, preferred_element_type=f32)
        return carry

    relays(3, *THIRD_B)
    lax.fori_loop(0, nfs, expand, 0)
    relays(3, *THIRD_C)
    for step in range(4, nz):
        relays(step, 0, pieces, 0, pieces)
    for step in range(2, nz):
        relay_others(step, jnp.logical_not(end))
    for way in (1, -1):

        @pl.when(jnp.logical_and(valid(z - way), at_end(z - way)))
        def _():
            for p in range(cross_end, cross_inner):
                for k in range(1, nx):
                    wz(way, z - way, k, p, z - way, True).wait_recv()
            await_got(wz_recv.at[lax.rem(nz - way, nz) - 1, pieces], wall.at[pl.ds(0, (nx - 1) * (pieces - cross_inner))])

    await_got(t_recv.at[0], sums.at[pl.ds(0, nt - 1)])
    whole = sums[0]
    for k in range(1, nt):
        whole = whole + sums[k]
    entries = nfs * rows * nt
    gscale = (1.0 / (jnp.sqrt(whole[0] / (entries * cg)) + rms_floor))[0:1, 0:1]
    vscale = (1.0 / (jnp.sqrt(whole[1] / (entries * cv)) + rms_floor))[0:1, 0:1]

    at = pl.ds(pl.multiple_of(f * rows, rows), rows)
    gstep = updates[at, :cg] * gscale
    vstep = updates[at, cg:] * vscale
    gsteps[...] = gstep
    vsteps[...] = vstep
    new_gw[...] = gw[...] - learn_rate * gstep
    new_vw[...] = vw[...] - learn_rate * vstep

    def finish(j, p):
        at = pl.ds(pl.multiple_of(j * rows + p * part, part), part)
        held = wall[j * pieces + p].astype(f32)
        update = updates[at, :]
        gcopy[at, :] = (held[:, :cg] - learn_rate * (update[:, :cg] * gscale)).astype(bf16)
        vcopy[at, :] = (held[:, cg:] - learn_rate * (update[:, cg:] * vscale)).astype(bf16)

    def finish_block(j, lo, hi):
        def body(p, carry):
            finish(j, p)
            return carry

        lax.fori_loop(lo, hi, body, 0)

    for zi in range(nz):
        finish_block(zi * nx + x, 0, pieces)
    for k in range(1, nx):
        finish_block(z * nx + xpeer(k), 0, pieces)

    @pl.when(inner)
    def _():
        await_got(rz_send.at[0], zsrc.at[pl.ds(0, nz - 1)])
        for m in range(1, nx):
            await_got(rx_send.at[m - 1], rsrc.at[0])

    @pl.when(end)
    def _():
        await_got(hand_send.at[0], handed.at[pl.ds(0, nz - 1)])
        for m in range(1, nx):
            await_got(rx_send.at[m - 1], rsrc.at[0, 0])

    await_got(dz_send.at[0], dall.at[pl.ds(0, nz - 1)])
    for m in range(1, nx):
        await_got(dx_send.at[m - 1], dall.at[pl.ds(0, nz)])
    await_got(t_send.at[0], sums.at[pl.ds(0, nt - 1)])
    for step in range(max(nz - 1, 1)):
        sent(step)
    for step in range(1, nz):
        relay_others(step, end)
    if cross_end:
        for zi in range(1, nz):
            for k in range(1, nx):
                finish_block(zpeer(zi) * nx + xpeer(k), 0, cross_end)
    for step in range(1, nz):
        for p in range(cross_end, pieces):
            for way in (1, -1):
                src_z = z - way * step

                @pl.when(valid(src_z))
                def _():
                    for k in range(1, nx):
                        group = group_of(p)
                        whole_row = jnp.logical_not(at_end(src_z))
                        sem = wx_recv.at[k - 1, lax.rem(src_z - z + nz, nz) - 1, group]
                        if p == cross_end:
                            for case, first in ((at_end(src_z), cross_end), (whole_row, cross_inner)):
                                if step == 1 and case is not whole_row:
                                    continue

                                @pl.when(case)
                                def _():
                                    await_got(sem, wall.at[pl.ds(0, pieces - SINGLES - first)])

                        elif group:

                            @pl.when(jnp.logical_not(rides(step, p, src_z)))
                            def _():
                                await_got(sem, wall.at[p])

                        finish(src_z * nx + xpeer(k), p)

    if nz > 1:
        sent(nz - 1)


def put_kernel(*refs):
    count = (len(refs) - 1) // 2
    sem = refs[-1]
    copies = [pltpu.make_async_copy(refs[i], refs[count + i], sem.at[i]) for i in range(count)]
    for copy in copies:
        copy.start()
    for copy in copies:
        copy.wait()


def per_device(nz, nx, nt, xin, gcot, fcot, scot, lam, proj, gw, gm, gs, vw, vm, vs):
    nfs = nz * nx
    rows, cg = gw.shape
    cv = vw.shape[1]
    cols = cg + cv
    depth, rank = proj.shape
    share = rank // nfs
    pieces = min(PIECES, rows // PIECE_ROWS)
    part = rows // pieces
    dma = pltpu.SemaphoreType.DMA
    shape = jax.ShapeDtypeStruct
    vmem = lambda a: pltpu.VMEM(a.shape, a.dtype)
    results = [
        shape((rows, cg), f32),
        shape((rows, cg), f32),
        shape((depth, cg), bf16),
        shape(gm.shape, f32),
        shape(gs.shape, f32),
        shape((rows, cv), f32),
        shape((rows, cv), f32),
        shape((depth, cv), bf16),
        shape(vm.shape, f32),
        shape(vs.shape, f32),
    ]
    arrays = [xin, gcot, fcot, scot, lam, proj, gw, gm, gs, vw, vm, vs]
    alone = cv == VDIM
    arrays = [
        a if alone and a is lam else pltpu.with_memory_space_constraint(a, pltpu.HBM)
        for a in arrays
    ]
    anywhere = pl.BlockSpec(memory_space=pl.ANY)
    inside = pl.BlockSpec(memory_space=pltpu.VMEM)
    held = pl.pallas_call(
        functools.partial(kernel, nz, nx, nt),
        out_shape=[vmem(a) for a in results],
        in_specs=[
            pl.BlockSpec(memory_space=pltpu.SMEM) if alone and a is lam else anywhere
            for a in (xin, gcot, fcot, scot, lam, proj, gw, gm, gs, vw, vm, vs)
        ],
        out_specs=[inside] * 10,
        scratch_shapes=[
            pltpu.SMEM(lam.shape, lam.dtype),
            vmem(xin),
            vmem(gcot),
            vmem(fcot),
            vmem(scot),
            vmem(proj),
            vmem(gw),
            vmem(vw),
            vmem(gm),
            vmem(gs),
            vmem(vm),
            vmem(vs),
            pltpu.VMEM((nfs * pieces, part, cols), bf16),
            pltpu.VMEM((rank, depth), bf16),
            pltpu.VMEM((rank, rank), bf16),
            pltpu.VMEM((rank, rank), bf16),
            pltpu.VMEM((rank, cols), f32),
            pltpu.VMEM((depth, cols), f32),
            pltpu.VMEM((nx, nz, share, cols), bf16),
            pltpu.VMEM((nx - 1, nz, share, cols), bf16),
            pltpu.VMEM((nz, share, cols), bf16),
            pltpu.VMEM((nz - 2, share, cols), bf16),
            pltpu.VMEM((nz, nx, share, cols), bf16),
            pltpu.VMEM((share, cols), f32),
            pltpu.VMEM((nfs, share, cols), bf16),
            pltpu.VMEM((rank, cols), f32),
            pltpu.VMEM((nt, 2, 8, 128), f32),
            dma((8,)),
            dma((4, DEPTH)),
            dma((2, nz)),
            dma((nz - 1, pieces + 1)),
            dma((nz - 1, (nx - 1) * max(pieces * CROSS_INNER // PIECES, 1))),
            dma((nx - 1, nz)),
            dma((nx - 1, nz - 1, SINGLES + 1)),
            dma((nx - 1, pieces)),
            dma((nx - 1,)),
            dma((nx - 1, nz)),
            dma((1,)),
            dma((1,)),
            dma((1,)),
            dma((nz,)),
            dma((nx - 1,)),
            dma((nx - 1,)),
            dma((1,)),
            dma((1,)),
            pltpu.SemaphoreType.REGULAR((nz - 2,)),
            dma((1,)),
            dma((nz,)),
        ],
        compiler_params=pltpu.CompilerParams(
            collective_id=0, has_side_effects=True, vmem_limit_bytes=40 * 1024 * 1024
        ),
    )(*arrays)
    return tuple(
        pl.pallas_call(
            put_kernel,
            out_shape=results,
            in_specs=[inside] * 10,
            out_specs=[anywhere] * 10,
            scratch_shapes=[dma((10,))],
            compiler_params=pltpu.CompilerParams(vmem_limit_bytes=8 * 1024 * 1024),
        )(*held)
    )


def solution(mesh):
    nz, nx = factor_fs(mesh.shape["fs"])
    assert nz > 3 and nx > 1
    split, whole = P("fs", "tp"), P(None, "tp")
    placed = (P("fs", None), split, split, split, P("tp"), P()) + (split,) * 6
    return jax.shard_map(
        functools.partial(per_device, nz, nx, mesh.shape["tp"]),
        mesh=mesh,
        in_specs=placed,
        out_specs=(split, split, whole, split, split, split, split, whole, split, split),
        check_vma=False,
    )
```

time: 51.5 us -> 46.6 us (0.905)
  Pallas kernels: 50.7 us -> 45.8 us
    pallas_call x1, Pallas kernels: 48.4 us -> 43.5 us  [per_device(): pl.pallas_call(functools.partial(kernel, nz, nx, nt), out_shape=[vmem(a)...]
where the time goes in v3:
time: 46.6 us; the launch traced here: 46.5 us
  Pallas kernels  45.8 us (98%)
  between operations  0.66 us (1%)
    pallas_call x1, Pallas kernels, per_device(): pl.pallas_call(functools.partial(kernel, nz, nx, nt), out_shape=[vmem(a)...  43.5 us
    pallas_call x1, Pallas kernels, per_device(): pl.pallas_call(put_kernel, out_shape=results, in_specs=[inside] * 10, out...  2.32 us

profile of v3, /device:TPU:0, one launch (start us, length us, event | category | flops | bytes accessed | tf_op | source)
XLA Modules:
  0.0 46.5 jit_solution(4177546774099912814)
XLA Ops:
  0.6 43.5 %shard_map.195 = (f32[256,512]{1,0:T(8,128)S(1)}, f32[256,512]{1,0:T(8,128)S(1)}, bf16[2048,512]{1,0:T(8,128)(2,1)S(1)}, f32[32,512]{1,0:T(8,128)S(1)}, f32[32,5...) custom-call(bf16[2048,2048]{1,0:T(8,128)(2,1)} %x_hbm.1, ...), custom_call_target="tpu_custom_call" | custom-call | tf_op jit(solution)/shard_map/pallas_call | solution.py:759
  44.2 2.3 %shard_map.196 = (f32[256,512]{1,0:T(8,128)}, f32[256,512]{1,0:T(8,128)}, bf16[2048,512]{1,0:T(8,128)(2,1)}, f32[32,512]{1,0:T(8,128)}, f32[32,512]{1,0:T(8,128)...) custom-call(f32[256,512]{1,0:T(8,128)S(1)} %get-tuple-element.20.ref, ...), custom_call_target="tpu_custom_call" | custom-call | tf_op jit(solution)/shard_map/pallas_call | solution.py:822

commit v4 on v3

--- a/solution.py
+++ b/solution.py
@@ -18,12 +18,13 @@
 HOLD_X = 5
 HOLD_Z = 5
 FIRST_A = (0, 5, 0, 4)
-FIRST_B = (5, 8, 4, 6)
-FIRST_C = (8, 8, 6, 8)
-SECOND_A = (0, 7, 0, 3)
+FIRST_B = (5, 8, 4, 7)
+FIRST_C = (8, 8, 7, 8)
+SECOND = (0, 3, 0, 0)
+SECOND_A = (3, 7, 0, 3)
 SECOND_B = (7, 8, 3, 8)
-THIRD_A = (0, 4, 0, 4)
-THIRD_B = (4, 6, 4, 6)
+THIRD_A = (0, 3, 0, 3)
+THIRD_B = (3, 6, 3, 6)
 THIRD_C = (6, 8, 6, 8)
 
 moment_decay = 0.9
@@ -157,7 +158,7 @@
         pl.semaphore_signal(barrier, inc=1, device_id=(f, lax.rem(t + k, nt)), device_id_type=MESH)
 
     small = [
-        pltpu.make_async_copy(src, dst, in_sem.at[i])
+        pltpu.make_async_copy(src, dst, in_sem.at[(0, 1, 2, 0, 1, 2, 3, 3)[i]])
         for i, (src, dst) in enumerate(
             [
                 (gw_hbm, gw),
@@ -178,11 +179,15 @@
     def chunk_copies(c):
         at = pl.ds(c * tokens, tokens)
         return [
-            pltpu.make_async_copy(src.at[at], dst.at[at], x_sem.at[i, c % DEPTH])
-            for i, (src, dst) in enumerate(
-                [(x_hbm, xv), (gcot_hbm, gcv), (fcot_hbm, fcv), (scot_hbm, scv)]
-            )
+            pltpu.make_async_copy(src.at[at], dst.at[at], x_sem.at[c % DEPTH])
+            for src, dst in [(x_hbm, xv), (gcot_hbm, gcv), (fcot_hbm, fcv), (scot_hbm, scv)]
         ]
+
+    def await_chunk(c):
+        wide = tokens * (x_hbm.shape[1] + cg + 2 * cv)
+        assert wide % x_hbm.shape[1] == 0
+        at = pl.ds(0, wide // x_hbm.shape[1])
+        pltpu.make_async_copy(x_hbm.at[at], xv.at[at], x_sem.at[c % DEPTH]).wait()
 
     for copy in small[:3] + small[7:] + chunk_copies(0):
         copy.start()
@@ -223,7 +228,7 @@
     def wx(k, p, src_z, src_x, own):
         at = (src_z * nx + src_x) * pieces + p
         if own:
-            sem = wx_own.at[nx - k - 1, p]
+            sem = wx_own.at[nx - k - 1, int(p >= HOLD_X)]
         else:
             sem = wx_recv.at[nx - k - 1, lax.rem(src_z - z + nz, nz) - 1, group_of(p)]
         return pltpu.make_async_remote_copy(
@@ -310,9 +315,11 @@
                     relay(step, k, p, where)
 
     def turns(lo, hi):
-        for p in range(min(lo, pieces), min(hi, pieces)):
-            for k in range(1, nx):
-                await_got(wx_own.at[k - 1, p], wall.at[p])
+        lo, hi = min(lo, pieces), min(hi, pieces)
+        for k in range(1, nx):
+            if lo < hi:
+                await_got(wx_own.at[k - 1, int(lo >= HOLD_X)], wall.at[pl.ds(lo, hi - lo)])
+            for p in range(lo, hi):
 
                 @pl.when(rides(0, p, z))
                 def _():
@@ -378,9 +385,7 @@
     for h in range(cv // VDIM):
         lam = jnp.where(head == h, lam_ref[h], lam)
     for c in range(CHUNKS):
-        for copy in chunk_copies(c):
-            copy.wait()
-
+        await_chunk(c)
         if c + DEPTH < CHUNKS:
             for copy in chunk_copies(c + DEPTH):
                 copy.start()
@@ -506,6 +511,7 @@
 
     pl.when(inner)(rest_over)
     relays(1, *FIRST_B)
+    relays(2, *SECOND)
     for i in range(3, 7):
         small[i].wait()
     row_sum(z)
@@ -570,8 +576,10 @@
             dx(m, zpeer(k), x).start()
     relays(2, *SECOND_B)
     turns(HOLD_X, pieces)
-    relay_others(1, jnp.logical_not(end))
+    relay_others(1, inner)
     relays(3, *THIRD_A)
+    for step in range(2, nz):
+        relay_others(step, inner)
     for m in range(1, nx):
         await_got(dx_recv.at[m - 1], dall.at[pl.ds(0, nz)])
 
@@ -607,13 +615,12 @@
         updates[at, :] = jnp.dot(pv[at, :], direction, preferred_element_type=f32)
         return carry
 
+    lax.fori_loop(0, nfs // 2, expand, 0, unroll=2)
     relays(3, *THIRD_B)
-    lax.fori_loop(0, nfs, expand, 0)
+    lax.fori_loop(nfs // 2, nfs, expand, 0, unroll=2)
     relays(3, *THIRD_C)
     for step in range(4, nz):
         relays(step, 0, pieces, 0, pieces)
-    for step in range(2, nz):
-        relay_others(step, jnp.logical_not(end))
     for way in (1, -1):
 
         @pl.when(jnp.logical_and(valid(z - way), at_end(z - way)))
@@ -651,7 +658,7 @@
             finish(j, p)
             return carry
 
-        lax.fori_loop(lo, hi, body, 0)
+        lax.fori_loop(lo, hi, body, 0, unroll=True)
 
     for zi in range(nz):
         finish_block(zi * nx + x, 0, pieces)
@@ -792,14 +799,14 @@
             pltpu.VMEM((nfs, share, cols), bf16),
             pltpu.VMEM((rank, cols), f32),
             pltpu.VMEM((nt, 2, 8, 128), f32),
-            dma((8,)),
-            dma((4, DEPTH)),
+            dma((4,)),
+            dma((DEPTH,)),
             dma((2, nz)),
             dma((nz - 1, pieces + 1)),
             dma((nz - 1, (nx - 1) * max(pieces * CROSS_INNER // PIECES, 1))),
             dma((nx - 1, nz)),
             dma((nx - 1, nz - 1, SINGLES + 1)),
-            dma((nx - 1, pieces)),
+            dma((nx - 1, 2)),
             dma((nx - 1,)),
             dma((nx - 1, nz)),
             dma((1,)),

time: 46.6 us -> 45.3 us (0.972)
  Pallas kernels: 45.8 us -> 44.5 us
    pallas_call x1, Pallas kernels: 43.5 us -> 42.2 us  [per_device(): pl.pallas_call(functools.partial(kernel, nz, nx, nt), out_shape=[vmem(a)...]
where the time goes in v4:
time: 45.3 us; the launch traced here: 45.1 us
  Pallas kernels  44.5 us (98%)
  between operations  0.66 us (1%)
    pallas_call x1, Pallas kernels, per_device(): pl.pallas_call(functools.partial(kernel, nz, nx, nt), out_shape=[vmem(a)...  42.2 us
    pallas_call x1, Pallas kernels, per_device(): pl.pallas_call(put_kernel, out_shape=results, in_specs=[inside] * 10, out...  2.32 us

profile of v4, /device:TPU:0, one launch (start us, length us, event | category | flops | bytes accessed | tf_op | source)
XLA Modules:
  0.0 45.1 jit_solution(2048241511406104148)
XLA Ops:
  0.6 42.2 %shard_map.195 = (f32[256,512]{1,0:T(8,128)S(1)}, f32[256,512]{1,0:T(8,128)S(1)}, bf16[2048,512]{1,0:T(8,128)(2,1)S(1)}, f32[32,512]{1,0:T(8,128)S(1)}, f32[32,5...) custom-call(bf16[2048,2048]{1,0:T(8,128)(2,1)} %x_hbm.1, ...), custom_call_target="tpu_custom_call" | custom-call | tf_op jit(solution)/shard_map/pallas_call | solution.py:766
  42.8 2.3 %shard_map.196 = (f32[256,512]{1,0:T(8,128)}, f32[256,512]{1,0:T(8,128)}, bf16[2048,512]{1,0:T(8,128)(2,1)}, f32[32,512]{1,0:T(8,128)}, f32[32,512]{1,0:T(8,128)...) custom-call(f32[256,512]{1,0:T(8,128)S(1)} %get-tuple-element.20.ref, ...), custom_call_target="tpu_custom_call" | custom-call | tf_op jit(solution)/shard_map/pallas_call | solution.py:829

commit v5 on v4

--- a/solution.py
+++ b/solution.py
@@ -10,7 +10,7 @@
 VDIM = 128
 PIECES = 8
 PIECE_ROWS = 16
-CROSS_END = 1
+CROSS_END = 2
 CROSS_INNER = 1
 CHUNKS = 4
 DEPTH = 3
@@ -20,8 +20,8 @@
 FIRST_A = (0, 5, 0, 4)
 FIRST_B = (5, 8, 4, 7)
 FIRST_C = (8, 8, 7, 8)
-SECOND = (0, 3, 0, 0)
-SECOND_A = (3, 7, 0, 3)
+SECOND = (0, 4, 0, 0)
+SECOND_A = (4, 7, 0, 3)
 SECOND_B = (7, 8, 3, 8)
 THIRD_A = (0, 3, 0, 3)
 THIRD_B = (3, 6, 3, 6)
@@ -134,6 +134,8 @@
     tokens = x_hbm.shape[0] // CHUNKS
     cross_end = pieces * CROSS_END // PIECES
     cross_inner = pieces * CROSS_INNER // PIECES
+    cross_most = max(cross_end, cross_inner)
+    cross_least = min(cross_end, cross_inner)
     items = [(k, p) for k in range(nx) for p in range(pieces)]
 
     def zpeer(k):
@@ -200,20 +202,19 @@
         at = pl.ds(p * part, part)
         wall[f * pieces + p, :, :cg] = gw[at, :].astype(bf16)
         wall[f * pieces + p, :, cg:] = vw[at, :].astype(bf16)
-
     def at_end(row):
         return jnp.logical_or(row == 0, row == nz - 1)
 
     def crosses(p, row):
-        return jnp.logical_or(p < cross_end, jnp.logical_and(p < cross_inner, jnp.logical_not(at_end(row))))
+        return jnp.where(at_end(row), p < cross_end, p < cross_inner)
 
     def wz(way, src_z, k, p, peer, here=False):
         at = (src_z * nx + xpeer(k)) * pieces + p
         away = lax.rem(src_z - (z if here else peer) + nz, nz) - 1
-        if k and p >= cross_inner:
+        if k and p >= cross_most:
             sem = wz_recv.at[away, pieces]
         elif k:
-            sem = wz_more.at[away, (k - 1) * max(cross_inner, 1) + p]
+            sem = wz_more.at[away, (k - 1) * max(cross_most, 1) + p]
         else:
             sem = wz_recv.at[away, p]
         return pltpu.make_async_remote_copy(
@@ -310,7 +311,7 @@
 
     def relay_others(step, where):
         if step < nz:
-            for p in range(cross_inner):
+            for p in range(cross_most):
                 for k in range(1, nx):
                     relay(step, k, p, where)
 
@@ -376,7 +377,6 @@
 
         if p < HOLD_X:
             over(z, p, True)
-
     for copy in small[2:3] + small[7:]:
         copy.wait()
     proj_t[...] = pv[...].T
@@ -485,7 +485,6 @@
 
     for k in range(1, nx):
         rx(k, z).start()
-
     def rest_over():
         for p in range(min(HOLD_X, pieces), pieces):
             over(z, p, True)
@@ -501,7 +500,6 @@
     gram = jnp.dot(proj_t[...], pv[...], preferred_element_type=f32)
     gram_high[...] = gram.astype(bf16)
     gram_low[...] = (gram - gram_high[...].astype(f32)).astype(bf16)
-
     @pl.when(inner)
     def _():
         for j in far:
@@ -529,7 +527,6 @@
         @pl.when(z != row)
         def _():
             low[...] += rsz[row - 1].astype(f32)
-
     for first, second, new_m, new_s, at in (
         (gm, gs, new_gm, new_gs, slice(0, cg)),
         (vm, vs, new_vm, new_vs, slice(cg, cols)),
@@ -582,7 +579,6 @@
         relay_others(step, inner)
     for m in range(1, nx):
         await_got(dx_recv.at[m - 1], dall.at[pl.ds(0, nz)])
-
     for j in range(nfs):
         dcat[pl.ds(j * share, share), :] = dall[j].astype(f32)
     direction = dcat[...].astype(bf16)
@@ -609,7 +605,6 @@
 
     for k in range(1, nt):
         tp(k, t).start()
-
     def expand(j, carry):
         at = pl.ds(pl.multiple_of(j * rows, rows), rows)
         updates[at, :] = jnp.dot(pv[at, :], direction, preferred_element_type=f32)
@@ -625,11 +620,10 @@
 
         @pl.when(jnp.logical_and(valid(z - way), at_end(z - way)))
         def _():
-            for p in range(cross_end, cross_inner):
+            for p in range(cross_end, cross_most):
                 for k in range(1, nx):
                     wz(way, z - way, k, p, z - way, True).wait_recv()
-            await_got(wz_recv.at[lax.rem(nz - way, nz) - 1, pieces], wall.at[pl.ds(0, (nx - 1) * (pieces - cross_inner))])
-
+            await_got(wz_recv.at[lax.rem(nz - way, nz) - 1, pieces], wall.at[pl.ds(0, (nx - 1) * (pieces - cross_most))])
     await_got(t_recv.at[0], sums.at[pl.ds(0, nt - 1)])
     whole = sums[0]
     for k in range(1, nt):
@@ -685,12 +679,12 @@
         sent(step)
     for step in range(1, nz):
         relay_others(step, end)
-    if cross_end:
+    if cross_least:
         for zi in range(1, nz):
             for k in range(1, nx):
-                finish_block(zpeer(zi) * nx + xpeer(k), 0, cross_end)
+                finish_block(zpeer(zi) * nx + xpeer(k), 0, cross_least)
     for step in range(1, nz):
-        for p in range(cross_end, pieces):
+        for p in range(cross_least, pieces):
             for way in (1, -1):
                 src_z = z - way * step
 
@@ -700,7 +694,7 @@
                         group = group_of(p)
                         whole_row = jnp.logical_not(at_end(src_z))
                         sem = wx_recv.at[k - 1, lax.rem(src_z - z + nz, nz) - 1, group]
-                        if p == cross_end:
+                        if p == cross_least:
                             for case, first in ((at_end(src_z), cross_end), (whole_row, cross_inner)):
                                 if step == 1 and case is not whole_row:
                                     continue
@@ -716,7 +710,6 @@
                                 await_got(sem, wall.at[p])
 
                         finish(src_z * nx + xpeer(k), p)
-
     if nz > 1:
         sent(nz - 1)
 
@@ -803,7 +796,7 @@
             dma((DEPTH,)),
             dma((2, nz)),
             dma((nz - 1, pieces + 1)),
-            dma((nz - 1, (nx - 1) * max(pieces * CROSS_INNER // PIECES, 1))),
+            dma((nz - 1, (nx - 1) * max(pieces * max(CROSS_INNER, CROSS_END) // PIECES, 1))),
             dma((nx - 1, nz)),
             dma((nx - 1, nz - 1, SINGLES + 1)),
             dma((nx - 1, 2)),

time: 45.3 us -> 45.3 us (level)
  no operation moved by 1% of the time
where the time goes in v5:
time: 45.3 us; the launch traced here: 45.2 us
  Pallas kernels  44.5 us (98%)
  between operations  0.66 us (1%)
    pallas_call x1, Pallas kernels, per_device(): pl.pallas_call(functools.partial(kernel, nz, nx, nt), out_shape=[vmem(a)...  42.2 us
    pallas_call x1, Pallas kernels, per_device(): pl.pallas_call(put_kernel, out_shape=results, in_specs=[inside] * 10, out...  2.32 us

profile of v5, /device:TPU:0, one launch (start us, length us, event | category | flops | bytes accessed | tf_op | source)
XLA Modules:
  0.0 45.2 jit_solution(15701699855522012378)
XLA Ops:
  0.6 42.2 %shard_map.195 = (f32[256,512]{1,0:T(8,128)S(1)}, f32[256,512]{1,0:T(8,128)S(1)}, bf16[2048,512]{1,0:T(8,128)(2,1)S(1)}, f32[32,512]{1,0:T(8,128)S(1)}, f32[32,5...) custom-call(bf16[2048,2048]{1,0:T(8,128)(2,1)} %x_hbm.1, ...), custom_call_target="tpu_custom_call" | custom-call | tf_op jit(solution)/shard_map/pallas_call | solution.py:759
  42.8 2.3 %shard_map.196 = (f32[256,512]{1,0:T(8,128)}, f32[256,512]{1,0:T(8,128)}, bf16[2048,512]{1,0:T(8,128)(2,1)}, f32[32,512]{1,0:T(8,128)}, f32[32,512]{1,0:T(8,128)...) custom-call(f32[256,512]{1,0:T(8,128)S(1)} %get-tuple-element.20.ref, ...), custom_call_target="tpu_custom_call" | custom-call | tf_op jit(solution)/shard_map/pallas_call | solution.py:822
